TPU v7x, 32 devices: a whole 2x2x4 slice. The times are simulated.
32 devices in a mesh: grp: 2 (over x), sp: 4 (over z), tp: 4 (over y, core).
Axes of the slice: x: 2, y: 2, z: 4, core: 2. Of those that a mesh axis runs over, the one named last changes fastest.
Arguments:
- stream: bfloat16 [4096, 2560], P(None, ('grp', 'sp')), parts along dimension 1, may hold values from -6 to 6
- norm_gain: float32 [2, 4096], replicated, may hold values from 0.1 to 1.9
- value_weight: bfloat16 [2, 2048, 4096], P(None, 'tp'), may hold values from -0.09375 to 0.09375
- gate_weight: bfloat16 [2, 2048, 4096], P(None, 'tp'), may hold values from -0.09375 to 0.09375
- conv_kernel: float32 [2, 2048, 31], P(None, 'tp')
- conv_bias: float32 [2, 2048], P(None, 'tp'), may hold values from -3 to 3
- channel_gain: float32 [2, 2048], P(None, 'tp'), may hold values from 0.1 to 1.9
- channel_bias: float32 [2, 2048], P(None, 'tp'), may hold values from -3 to 3
- out_weight: bfloat16 [2, 4096, 2048], P(None, 'tp'), may hold values from -0.25 to 0.25
Outputs:
- result: bfloat16 [4096, 2560], P('tp', ('grp', 'sp')), parts along dimension 1
There are 2 independent parts, one for each index of `grp`. A program takes and returns all parts, laid end to end along the dimension named above; an argument that names none is the same for every part. Nothing has to cross between parts.
All inputs are finite; a program needn't handle non-finite values.
Results may differ from a plain program's by a relative error of at most 0.012.
Values may be sent and summed in bfloat16 or wider, within the bound.
A program may use at most 128 MiB of HBM per device.

v0:
```python
import functools

import jax
import jax.numpy as jnp
from jax import lax
from jax.experimental import pallas as pl
from jax.experimental.pallas import tpu as pltpu
from jax.sharding import PartitionSpec as P

K = 31
LAYERS = 2


epsilon = 1e-06


def shifted(value, axis, steps):
    count = lax.axis_size(axis)
    initial, last = (max(0, -steps), min(count, count - steps))
    return lax.ppermute(value, axis, [(source, source + steps) for source in range(initial, last)])


def depthwise(signal, kernel):
    out = lax.conv_general_dilated(
        signal[None],
        kernel[:, None, :],
        (1,),
        [(0, 0)],
        dimension_numbers=("NCW", "OIW", "NCW"),
        feature_group_count=kernel.shape[0],
        precision=lax.Precision.HIGHEST,
    )
    return out[0]


def norm_project(whole, gain, weights):
    scaling = lax.rsqrt(jnp.mean(whole * whole, axis=0, keepdims=True) + epsilon)
    normed = (whole * scaling * gain[:, None]).astype(jnp.bfloat16)
    return jnp.dot(weights, normed, preferred_element_type=jnp.float32)


def local(
    stream,
    norm_gain,
    value_weight,
    gate_weight,
    conv_kernel,
    conv_bias,
    channel_gain,
    channel_bias,
    out_weight,
):
    shard_channels = value_weight.shape[1]
    total_channels = shard_channels * lax.axis_size("tp")
    shard_features = out_weight.shape[1]
    tokens_here = stream.shape[1]
    row_start = lax.axis_index("tp") * shard_features
    whole = stream.astype(jnp.float32)
    current = lax.dynamic_slice_in_dim(whole, row_start, shard_features, 0)
    layer_out = stream
    for layer in range(LAYERS):
        both_weights = jnp.concatenate((value_weight[layer], gate_weight[layer]), axis=0)
        if layer == 0:
            projected = norm_project(whole, norm_gain[layer], both_weights)
        else:
            gathered = lax.all_gather(layer_out, "tp", axis=0, tiled=True).astype(jnp.float32)
            projected = norm_project(gathered, norm_gain[layer], both_weights)
        gated = (projected[:shard_channels] * jax.nn.sigmoid(projected[shard_channels:])).astype(
            jnp.bfloat16
        )
        earlier = shifted(gated[:, tokens_here - (K - 1) :], "sp", 1)
        extended = jnp.concatenate((earlier, gated), axis=1).astype(jnp.float32)
        filtered = depthwise(extended, conv_kernel[layer]) + conv_bias[layer][:, None]
        first_sum, square_sum = lax.psum(
            (
                jnp.sum(filtered, axis=0, keepdims=True),
                jnp.sum(filtered * filtered, axis=0, keepdims=True),
            ),
            "tp",
        )
        row_mean = first_sum / total_channels
        centred = filtered - row_mean
        spread = square_sum / total_channels - row_mean * row_mean
        activated = jax.nn.silu(
            centred * lax.rsqrt(spread + epsilon) * channel_gain[layer][:, None]
            + channel_bias[layer][:, None]
        ).astype(jnp.bfloat16)

        def accumulate(total, piece, start, weights=out_weight[layer]):
            weight_cols = lax.dynamic_slice_in_dim(weights, start, piece.shape[0], 1)
            return total + jnp.dot(weight_cols, piece, preferred_element_type=jnp.float32)

        zero_branch = jnp.zeros((shard_features, tokens_here), jnp.float32)
        branch = accumulate(
            zero_branch, lax.all_gather(activated, "tp", axis=0, tiled=True), jnp.int32(0)
        )
        layer_out = (current + branch).astype(jnp.bfloat16)
        current = layer_out.astype(jnp.float32)
    return layer_out


MESH = pl.DeviceIdType.MESH
LANES = 128
CHUNK = 256
HALO = 32
ROWS = 64
CORES = 2
WEIGHT_PIECES = 4


def dot_nt(left, right):
    return lax.dot_general(
        left, right, (((1,), (1,)), ((), ())), preferred_element_type=jnp.float32
    )


def kernel(
    n_tp,
    n_sp,
    x_ref,
    gain_ref,
    taps_ref,
    bias_ref,
    chan_gain_ref,
    chan_bias_ref,
    wv_ref,
    wg_ref,
    ow_ref,
    out_ref,
    wp,
    wo,
    xg,
    ext,
    filt,
    taps,
    norm_squares,
    part,
    column,
    halo_out,
    halo_in,
    stat,
    ag,
    sg,
    accp,
    acco,
    res,
    wp_sem,
    wo_sem,
    halo_send,
    halo_recv,
    stat_send,
    stat_recv,
    y_send,
    y_recv,
    f_send,
    f_recv,
):
    tokens, width = x_ref.shape
    chans = wv_ref.shape[1]
    feats = ow_ref.shape[1]
    total_chans = chans * n_tp
    n_y = n_tp // CORES
    piece = width // WEIGHT_PIECES
    padded = part.shape[2]
    split = (tokens // 2 - HALO) // HALO * HALO
    spans = (
        ((split, tokens), (0, split)),
        ((split + HALO, tokens), (0, split + HALO)),
    )
    me = lax.axis_index("tp")
    sp = lax.axis_index("sp")
    my_y, core = me // CORES, me % CORES
    sibling = my_y * CORES + (1 - core)

    def tp_id(index):
        return {"tp": index}

    barrier = pltpu.get_barrier_semaphore()
    for step in range(1, n_tp):
        pl.semaphore_signal(
            barrier, inc=1, device_id=tp_id(lax.rem(me + step, n_tp)), device_id_type=MESH
        )

    @pl.when(sp > 0)
    def _():
        pl.semaphore_signal(barrier, inc=1, device_id={"sp": sp - 1}, device_id_type=MESH)

    @pl.when(sp < n_sp - 1)
    def _():
        pl.semaphore_signal(barrier, inc=1, device_id={"sp": sp + 1}, device_id_type=MESH)

    def proj_copies(layer, index):
        cols = pl.ds(index * piece, piece)
        return [
            pltpu.make_async_copy(
                ref.at[layer, :, cols], wp.at[layer, half, :, cols], wp_sem.at[layer, index]
            )
            for half, ref in enumerate((wv_ref, wg_ref))
        ]

    def out_copy(layer):
        return pltpu.make_async_copy(ow_ref.at[layer], wo.at[layer], wo_sem.at[layer])

    for layer in range(LAYERS):
        for index in range(WEIGHT_PIECES):
            for copy in proj_copies(layer, index):
                copy.start()
        out_copy(layer).start()

    for layer in range(LAYERS):
        taps[layer] = taps_ref[:, layer, :]

    def prepare(layer, read, first_col, cols, span, at, first):
        gains = gain_ref[layer : layer + 1, pl.ds(first_col, cols)]

        @pl.loop(0, (span[1] - span[0]) // ROWS)
        def _(block):
            rows = pl.ds(pl.multiple_of(span[0] + block * ROWS, HALO), ROWS)
            squares = jnp.zeros((ROWS, LANES), jnp.float32)
            if not first:
                squares = norm_squares[rows, :]
            for lane in range(cols // LANES):
                here = slice(lane * LANES, (lane + 1) * LANES)
                values = read(rows, here).astype(jnp.float32)
                squares = squares + values * values
                xg[rows, at + here.start : at + here.stop] = (values * gains[:, here]).astype(
                    jnp.bfloat16
                )
            norm_squares[rows, :] = squares

    def project(layer, first_col, cols, span, first):
        rows = slice(*span)
        for half in range(2):
            held = slice(half * chans, (half + 1) * chans)
            product = dot_nt(xg[rows, :cols], wp[layer, half, :, pl.ds(first_col, cols)])
            if first:
                accp[rows, held] = product
            else:
                accp[rows, held] += product

    pending = []

    def remote(source, target, send, recv, device):
        copy = pltpu.make_async_remote_copy(
            src_ref=source,
            dst_ref=target,
            send_sem=send,
            recv_sem=recv,
            device_id=tp_id(device),
            device_id_type=MESH,
        )
        return copy

    def y_copy(phase, buf, step, chunk, owner, rows):
        target = lax.rem(my_y + step, n_y) * CORES + core
        ref = buf.at[owner, chunk, rows]
        return remote(
            ref, ref, y_send.at[phase, step, chunk], y_recv.at[phase, step, chunk], target
        )

    def f_copy(phase, buf, step, chunk, owner, rows):
        ref = buf.at[owner, chunk, rows]
        return remote(
            ref, ref, f_send.at[phase, step, chunk], f_recv.at[phase, step, chunk], sibling
        )

    def send_own(phase, buf, chunk, span):
        rows = pl.ds(span[0], span[1] - span[0])
        for step in range(1, n_y):
            copy = y_copy(phase, buf, step, chunk, me, rows)
            copy.start()
            pending.append(copy)
        copy = f_copy(phase, buf, 0, chunk, me, rows)
        copy.start()
        pending.append(copy)

    def near(phase, buf, chunks, span, use):
        rows = pl.ds(span[0], span[1] - span[0])
        use(me, range(chunks), span, True)
        for chunk in range(chunks):
            f_copy(phase, buf, 0, chunk, sibling, rows).wait_recv()
        use(sibling, range(chunks), span, False)

    def arrive(phase, buf, chunk, span, use):
        rows = pl.ds(span[0], span[1] - span[0])
        for step in range(1, n_y):
            owner = lax.rem(my_y + n_y - step, n_y) * CORES + core
            y_copy(phase, buf, step, chunk, owner, rows).wait_recv()
            copy = f_copy(phase, buf, step, chunk, owner, rows)
            copy.start()
            pending.append(copy)
            use(owner, (chunk,), span, False)

    def relayed(phase, buf, chunk, span, use):
        rows = pl.ds(span[0], span[1] - span[0])
        for step in range(1, n_y):
            owner = lax.rem(my_y + n_y - step, n_y) * CORES + 1 - core
            f_copy(phase, buf, step, chunk, owner, rows).wait_recv()
            use(owner, (chunk,), span, False)

    def far(phase, buf, chunks, span, use):
        for chunk in chunks:
            arrive(phase, buf, chunk, span, use)
            if chunk > 0:
                relayed(phase, buf, chunk - 1, span, use)

    def gate(first_row, count):
        rows = pl.ds(first_row, count)
        scaling = lax.rsqrt(
            jnp.sum(norm_squares[rows, :], axis=1, keepdims=True) / width + epsilon
        )
        value = accp[rows, :chans] * scaling
        gates = accp[rows, chans:] * scaling
        gated = (value * jax.nn.sigmoid(gates)).astype(jnp.bfloat16)
        widened = gated.astype(jnp.float32)
        for lane in range(chans // LANES):
            ext[lane, pl.ds(first_row + HALO, count), :] = widened[
                :, lane * LANES : (lane + 1) * LANES
            ]
        return gated

    def gate_rows(start, stop):
        @pl.loop(0, (stop - start) // HALO)
        def _(block):
            gate(pl.multiple_of(start + block * HALO, HALO), HALO)

    def halo_copy(layer):
        return pltpu.make_async_remote_copy(
            src_ref=halo_out.at[layer],
            dst_ref=halo_in.at[layer],
            send_sem=halo_send.at[layer],
            recv_sem=halo_recv.at[layer],
            device_id={"sp": lax.rem(sp + 1, n_sp)},
            device_id_type=MESH,
        )

    def send_halo(layer):
        halo_out[layer] = gate(tokens - HALO, HALO)

        @pl.when(sp < n_sp - 1)
        def _():
            halo_copy(layer).start()

    def receive_halo(layer):
        @pl.when(sp > 0)
        def _():
            halo_copy(layer).wait_recv()
            for lane in range(chans // LANES):
                ext[lane, :HALO, :] = halo_in[
                    layer, :, lane * LANES : (lane + 1) * LANES
                ].astype(jnp.float32)

        @pl.when(sp == 0)
        def _():
            ext[:, :HALO, :] = jnp.zeros((chans // LANES, HALO, LANES), jnp.float32)

    def convolve(layer, half, start, stop):
        base = spans[layer][half][0]
        blocks = []
        while start < stop:
            count = min(ROWS, stop - start)
            blocks.append((start, count))
            start += count

        @pl.loop(0, chans // LANES)
        def _(lane):
            here = pl.ds(pl.multiple_of(lane * LANES, LANES), LANES)
            bias = bias_ref[layer : layer + 1, here]
            for first_row, count in blocks:
                rows = slice(first_row, first_row + count)
                total = jnp.broadcast_to(bias, (count, LANES))
                for tap in range(K):
                    begin = first_row + HALO - K + 1 + tap
                    window = ext[lane, begin : begin + count, :]
                    total = total + window * taps[layer, tap : tap + 1, here]
                filt[rows, here] = total
                inner = slice(first_row - base, first_row - base + count)
                part[half, 0, inner, :] += total
                part[half, 1, inner, :] += total * total

    def stat_copy(layer, half, step, owner, target):
        ref = stat.at[layer, half, owner]
        index = layer * 2 + half
        return remote(ref, ref, stat_send.at[index, step], stat_recv.at[index, step], target)

    def send_stats(layer, half):
        first_row = jnp.sum(jnp.transpose(part[half, 0]), axis=0, keepdims=True)
        square_row = jnp.sum(jnp.transpose(part[half, 1]), axis=0, keepdims=True)
        row_index = lax.broadcasted_iota(jnp.int32, (8, padded), 0)
        stat[layer, half, me] = jnp.where(row_index == 0, first_row, square_row)
        for step in range(1, n_tp):
            copy = stat_copy(layer, half, step, me, lax.rem(me + step, n_tp))
            copy.start()
            pending.append(copy)

    def activate(layer, half, phase):
        for step in range(1, n_tp):
            origin = lax.rem(me + n_tp - step, n_tp)
            stat_copy(layer, half, step, origin, origin).wait_recv()
        totals = jnp.sum(stat[layer, half], axis=0) / total_chans
        mean_row = totals[0:1]
        rstd_row = lax.rsqrt(totals[1:2] - mean_row * mean_row + epsilon)
        column[0] = jnp.transpose(jnp.broadcast_to(mean_row, (LANES, padded)))
        column[1] = jnp.transpose(jnp.broadcast_to(rstd_row, (LANES, padded)))
        start, stop = spans[layer][half]
        for chunk in range(chans // CHUNK):

            @pl.loop(0, (stop - start) // HALO)
            def _(block):
                inner = pl.ds(pl.multiple_of(block * HALO, HALO), HALO)
                rows = pl.ds(pl.multiple_of(start + block * HALO, HALO), HALO)
                for lane in range(CHUNK // LANES):
                    here = slice(chunk * CHUNK + lane * LANES, chunk * CHUNK + (lane + 1) * LANES)
                    values = (filt[rows, here] - column[0, inner, :]) * column[1, inner, :]
                    values = (
                        values * chan_gain_ref[layer : layer + 1, here]
                        + chan_bias_ref[layer : layer + 1, here]
                    )
                    ag[layer, me, chunk, rows, lane * LANES : (lane + 1) * LANES] = (
                        jax.nn.silu(values).astype(jnp.bfloat16)
                    )

            send_own(phase, ag.at[layer], chunk, (start, stop))

    def use_activated(layer):
        def use(owner, chunks, span, first):
            rows = slice(*span)
            total = res[rows, :] if first else acco[rows, :]
            for chunk in chunks:
                start = pl.multiple_of(owner * chans + chunk * CHUNK, LANES)
                total = total + dot_nt(
                    ag[layer, owner, chunk, rows, :], wo[layer, :, pl.ds(start, CHUNK)]
                )
            acco[rows, :] = total

        return use

    def use_stream(owner, chunks, span, first):
        start = pl.multiple_of(owner * feats + chunks[0] * CHUNK, LANES)
        for chunk in chunks:
            prepare(
                1,
                lambda rows, here: sg[owner, chunk, rows, here],
                pl.multiple_of(owner * feats + chunk * CHUNK, LANES),
                CHUNK,
                span,
                (chunk - chunks[0]) * CHUNK,
                first and chunk == 0,
            )
        project(1, start, len(chunks) * CHUNK, span, first)

    n_a, n_f = chans // CHUNK, feats // CHUNK
    part[...] = jnp.zeros(part.shape, jnp.float32)
    for index in range(WEIGHT_PIECES):
        start = index * piece
        prepare(
            0,
            lambda rows, here: x_ref[rows, start + here.start : start + here.stop],
            start,
            piece,
            (0, tokens),
            0,
            index == 0,
        )
        for copy in proj_copies(0, index):
            copy.wait()
        project(0, start, piece, (0, tokens), index == 0)
    res[...] = x_ref[:, pl.ds(pl.multiple_of(me * feats, LANES), feats)].astype(jnp.float32)
    pl.semaphore_wait(
        barrier,
        n_tp - 1 + jnp.where(sp > 0, 1, 0) + jnp.where(sp < n_sp - 1, 1, 0),
    )
    late, early = spans[0]
    send_halo(0)
    gate_rows(0, tokens - HALO)
    convolve(0, 0, *late)
    send_stats(0, 0)
    convolve(0, 1, ROWS, early[1])
    receive_halo(0)
    convolve(0, 1, 0, ROWS)
    send_stats(0, 1)
    activate(0, 0, 0)
    activate(0, 1, 1)
    out_copy(0).wait()
    def send_stream(half, span):
        rows = slice(*span)
        for chunk in range(n_f):
            here = slice(chunk * CHUNK, (chunk + 1) * CHUNK)
            rounded = acco[rows, here].astype(jnp.bfloat16)
            sg[me, chunk, rows, :] = rounded
            send_own(2 + half, sg, chunk, span)
            res[rows, here] = rounded.astype(jnp.float32)

    use = use_activated(0)
    near(0, ag.at[0], n_a, late, use)
    far(0, ag.at[0], range(n_a), late, use)
    near(1, ag.at[0], n_a, early, use)
    relayed(0, ag.at[0], n_a - 1, late, use)
    send_stream(0, late)
    far(1, ag.at[0], range(n_a), early, use)
    part[...] = jnp.zeros(part.shape, jnp.float32)
    for index in range(WEIGHT_PIECES):
        for copy in proj_copies(1, index):
            copy.wait()
    near(2, sg, n_f, late, use_stream)
    relayed(1, ag.at[0], n_a - 1, early, use)
    send_stream(1, early)
    far(2, sg, range(n_f), late, use_stream)
    near(3, sg, n_f, early, use_stream)
    relayed(2, sg, n_f - 1, late, use_stream)
    send_halo(1)
    gate_rows(split, tokens - HALO)
    convolve(1, 0, *spans[1][0])
    send_stats(1, 0)
    far(3, sg, range(n_f // 2), early, use_stream)
    activate(1, 0, 4)
    far(3, sg, range(n_f // 2, n_f), early, use_stream)
    relayed(3, sg, n_f - 1, early, use_stream)
    gate_rows(0, split)
    convolve(1, 1, HALO, spans[1][1][1])
    receive_halo(1)
    convolve(1, 1, 0, HALO)
    send_stats(1, 1)
    out_copy(1).wait()
    use = use_activated(1)
    near(4, ag.at[1], n_a, spans[1][0], use)
    activate(1, 1, 5)
    far(4, ag.at[1], range(n_a), spans[1][0], use)
    near(5, ag.at[1], n_a, spans[1][1], use)
    relayed(4, ag.at[1], n_a - 1, spans[1][0], use)
    far(5, ag.at[1], range(n_a), spans[1][1], use)
    relayed(5, ag.at[1], n_a - 1, spans[1][1], use)
    out_ref[...] = acco[...].astype(jnp.bfloat16)

    @pl.when(sp < n_sp - 1)
    def _():
        for layer in range(LAYERS):
            halo_copy(layer).wait_send()

    for copy in pending:
        copy.wait_send()


def fused(mesh, stream, norm_gain, value_weight, gate_weight, conv_kernel, conv_bias,
          channel_gain, channel_bias, out_weight):
    n_tp, n_sp = mesh.shape["tp"], mesh.shape["sp"]
    width, tokens = stream.shape
    chans, feats = value_weight.shape[1], out_weight.shape[1]
    fits = (
        n_tp % CORES == 0
        and chans % CHUNK == 0
        and feats % CHUNK == 0
        and width % (WEIGHT_PIECES * CHUNK) == 0
        and tokens % ROWS == 0
        and (tokens // 2 - HALO) // HALO * HALO % ROWS == 0
        and tokens >= 4 * ROWS
        and LAYERS == 2
        and n_tp <= 8
    )
    if not fits:
        return local(stream, norm_gain, value_weight, gate_weight, conv_kernel, conv_bias,
                     channel_gain, channel_bias, out_weight)
    split = (tokens // 2 - HALO) // HALO * HALO
    padded = -(-(tokens - split) // LANES) * LANES
    n_y = n_tp // CORES
    n_a, n_f = chans // CHUNK, feats // CHUNK
    most = max(n_a, n_f)
    f32, bf16 = jnp.float32, jnp.bfloat16
    vmem = pl.BlockSpec(memory_space=pltpu.VMEM)
    anyspace = pl.BlockSpec(memory_space=pl.ANY)
    out = pl.pallas_call(
        functools.partial(kernel, n_tp, n_sp),
        out_shape=jax.ShapeDtypeStruct((tokens, feats), bf16),
        in_specs=[vmem] * 6 + [anyspace, anyspace, anyspace],
        out_specs=vmem,
        scratch_shapes=[
            pltpu.VMEM((LAYERS, 2, chans, width), bf16),
            pltpu.VMEM((LAYERS, feats, chans * n_tp), bf16),
            pltpu.VMEM((tokens, max(width // WEIGHT_PIECES, feats)), bf16),
            pltpu.VMEM((chans // LANES, HALO + tokens, LANES), f32),
            pltpu.VMEM((tokens, chans), f32),
            pltpu.VMEM((LAYERS, K, chans), f32),
            pltpu.VMEM((tokens, LANES), f32),
            pltpu.VMEM((2, 2, padded, LANES), f32),
            pltpu.VMEM((2, padded, LANES), f32),
            pltpu.VMEM((LAYERS, HALO, chans), bf16),
            pltpu.VMEM((LAYERS, HALO, chans), bf16),
            pltpu.VMEM((LAYERS, 2, n_tp, 8, padded), f32),
            pltpu.VMEM((LAYERS, n_tp, n_a, tokens, CHUNK), bf16),
            pltpu.VMEM((n_tp, n_f, tokens, CHUNK), bf16),
            pltpu.VMEM((tokens, 2 * chans), f32),
            pltpu.VMEM((tokens, feats), f32),
            pltpu.VMEM((tokens, feats), f32),
            pltpu.SemaphoreType.DMA((LAYERS, WEIGHT_PIECES)),
            pltpu.SemaphoreType.DMA((LAYERS,)),
            pltpu.SemaphoreType.DMA((LAYERS,)),
            pltpu.SemaphoreType.DMA((LAYERS,)),
            pltpu.SemaphoreType.DMA((LAYERS * 2, n_tp)),
            pltpu.SemaphoreType.DMA((LAYERS * 2, n_tp)),
            pltpu.SemaphoreType.DMA((6, n_y, most)),
            pltpu.SemaphoreType.DMA((6, n_y, most)),
            pltpu.SemaphoreType.DMA((6, n_y, most)),
            pltpu.SemaphoreType.DMA((6, n_y, most)),
        ],
        compiler_params=pltpu.CompilerParams(
            collective_id=0, has_side_effects=True, vmem_limit_bytes=60 * 1024 * 1024
        ),
    )(stream.T, norm_gain, jnp.transpose(conv_kernel, (2, 0, 1)), conv_bias, channel_gain, channel_bias,
       value_weight, gate_weight, out_weight)
    return out.T


def solution(mesh):
    placed = (
        P(None, ("grp", "sp")),
        P(),
        P(None, "tp", None),
        P(None, "tp", None),
        P(None, "tp", None),
        P(None, "tp"),
        P(None, "tp"),
        P(None, "tp"),
        P(None, "tp", None),
    )
    return jax.shard_map(
        functools.partial(fused, mesh), mesh=mesh, in_specs=placed, out_specs=P("tp", ("grp", "sp")), check_vma=False
    )
```

profile of v0, /device:TPU:0, one launch (start us, length us, event | category | flops | bytes accessed | tf_op | source)
XLA Modules:
  0.0 57.0 jit_solution(17792574597654737181)
XLA Ops:
  0.0 55.0 %shard_map.91 = bf16[320,1024]{1,0:T(8,128)(2,1)} custom-call(bf16[320,4096]{1,0:T(8,128)(2,1)} %bitcast.3, f32[2,4096]{1,0:T(2,128)} %gain_ref.1, f32[31,2,512]{2,1,0:T(2,128)} %bitcast.5, f32[2,512]{1,0:T(2,128)} %bias_ref.1, f32[2,512]{1,0:T(2,128)} %chan_gain_ref.1, f32[2,512]{1,0:T(2,128)} %chan_bias_ref.1, bf16[2,512,4096]{2,1,0:T(8,128)(2,1)} %wv_ref.1, ...), custom_call_target="tpu_custom_call" | custom-call | tf_op jit(solution)/shard_map/pallas_call | solution.py:571
  55.0 2.0 %copy.11 = bf16[1024,320]{0,1:T(8,128)(2,1)} copy(bf16[1024,320]{0,1:T(8,128)(2,1)} %bitcast.4) | data formatting | bytes 1310720
where the time goes:
time: 57.5 us; the launch traced here: 57 us
  Pallas kernels  55 us (96%)
  local copies, waits for them, and re-layouts  1.97 us (3%)
    pallas_call x1, Pallas kernels, fused(): pl.pallas_call(functools.partial(kernel, n_tp, n_sp), out_shape=jax.Shape...  55 us
    unnamed x1, local copies, waits for them, and re-layouts  1.97 us

commit v1 on v0

v1 whole, which is shorter than its diff:
```python
import functools

import jax
import jax.numpy as jnp
from jax import lax
from jax.experimental import pallas as pl
from jax.experimental.pallas import tpu as pltpu
from jax.sharding import PartitionSpec as P

K = 31
LAYERS = 2


epsilon = 1e-06


def shifted(value, axis, steps):
    count = lax.axis_size(axis)
    initial, last = (max(0, -steps), min(count, count - steps))
    return lax.ppermute(value, axis, [(source, source + steps) for source in range(initial, last)])


def depthwise(signal, kernel):
    out = lax.conv_general_dilated(
        signal[None],
        kernel[:, None, :],
        (1,),
        [(0, 0)],
        dimension_numbers=("NCW", "OIW", "NCW"),
        feature_group_count=kernel.shape[0],
        precision=lax.Precision.HIGHEST,
    )
    return out[0]


def norm_project(whole, gain, weights):
    scaling = lax.rsqrt(jnp.mean(whole * whole, axis=0, keepdims=True) + epsilon)
    normed = (whole * scaling * gain[:, None]).astype(jnp.bfloat16)
    return jnp.dot(weights, normed, preferred_element_type=jnp.float32)


def local(
    stream,
    norm_gain,
    value_weight,
    gate_weight,
    conv_kernel,
    conv_bias,
    channel_gain,
    channel_bias,
    out_weight,
):
    shard_channels = value_weight.shape[1]
    total_channels = shard_channels * lax.axis_size("tp")
    shard_features = out_weight.shape[1]
    tokens_here = stream.shape[1]
    row_start = lax.axis_index("tp") * shard_features
    whole = stream.astype(jnp.float32)
    current = lax.dynamic_slice_in_dim(whole, row_start, shard_features, 0)
    layer_out = stream
    for layer in range(LAYERS):
        both_weights = jnp.concatenate((value_weight[layer], gate_weight[layer]), axis=0)
        if layer == 0:
            projected = norm_project(whole, norm_gain[layer], both_weights)
        else:
            gathered = lax.all_gather(layer_out, "tp", axis=0, tiled=True).astype(jnp.float32)
            projected = norm_project(gathered, norm_gain[layer], both_weights)
        gated = (projected[:shard_channels] * jax.nn.sigmoid(projected[shard_channels:])).astype(
            jnp.bfloat16
        )
        earlier = shifted(gated[:, tokens_here - (K - 1) :], "sp", 1)
        extended = jnp.concatenate((earlier, gated), axis=1).astype(jnp.float32)
        filtered = depthwise(extended, conv_kernel[layer]) + conv_bias[layer][:, None]
        first_sum, square_sum = lax.psum(
            (
                jnp.sum(filtered, axis=0, keepdims=True),
                jnp.sum(filtered * filtered, axis=0, keepdims=True),
            ),
            "tp",
        )
        row_mean = first_sum / total_channels
        centred = filtered - row_mean
        spread = square_sum / total_channels - row_mean * row_mean
        activated = jax.nn.silu(
            centred * lax.rsqrt(spread + epsilon) * channel_gain[layer][:, None]
            + channel_bias[layer][:, None]
        ).astype(jnp.bfloat16)

        def accumulate(total, piece, start, weights=out_weight[layer]):
            weight_cols = lax.dynamic_slice_in_dim(weights, start, piece.shape[0], 1)
            return total + jnp.dot(weight_cols, piece, preferred_element_type=jnp.float32)

        zero_branch = jnp.zeros((shard_features, tokens_here), jnp.float32)
        branch = accumulate(
            zero_branch, lax.all_gather(activated, "tp", axis=0, tiled=True), jnp.int32(0)
        )
        layer_out = (current + branch).astype(jnp.bfloat16)
        current = layer_out.astype(jnp.float32)
    return layer_out


MESH = pl.DeviceIdType.MESH
LANES = 128
SUBLANES = 8
CHUNK = 256
HALO = 32
ROWS = 64
CORES = 2
PIECES = 4


def dot_nt(left, right):
    return lax.dot_general(
        left, right, (((1,), (1,)), ((), ())), preferred_element_type=jnp.float32
    )


def kernel(
    n_tp,
    n_sp,
    split,
    x_hbm,
    gain_hbm,
    taps_hbm,
    bias_hbm,
    chan_gain_hbm,
    chan_bias_hbm,
    wv_ref,
    wg_ref,
    ow_ref,
    out_ref,
    gain_ref,
    raw_taps,
    bias_ref,
    chan,
    wp,
    wo,
    x_in,
    xg,
    ext,
    filt,
    taps,
    norm_squares,
    scale,
    part,
    columns,
    halo_out,
    halo_in,
    stat,
    square,
    cf,
    ag,
    sg,
    accp,
    acco,
    res,
    small_sem,
    x_sem,
    wp_sem,
    wo_sem,
    chan_send,
    chan_recv,
    halo_send,
    halo_recv,
    stat_send,
    stat_recv,
    square_send,
    square_recv,
    y_send,
    y_recv,
    f_send,
    f_recv,
):
    tokens, width = x_in.shape
    chans = wv_ref.shape[1]
    feats = ow_ref.shape[1]
    total_chans = chans * n_tp
    n_y = n_tp // CORES
    piece = width // PIECES
    padded = stat.shape[-1]
    n_a, n_f = chans // CHUNK, feats // CHUNK
    groups = CHUNK // LANES
    spans = (
        ((split, tokens), (0, split)),
        ((split + HALO, tokens), (0, split + HALO)),
    )
    me = lax.axis_index("tp")
    sp = lax.axis_index("sp")
    my_y, core = me // CORES, me % CORES
    sibling = my_y * CORES + (1 - core)

    def tp_id(index):
        return {"tp": index}

    smalls = [
        pltpu.make_async_copy(source, target, small_sem.at[index])
        for index, (source, target) in enumerate(
            (
                (gain_hbm, gain_ref),
                (taps_hbm, raw_taps),
                (bias_hbm, bias_ref),
                (chan_gain_hbm, chan.at[my_y, 0]),
                (chan_bias_hbm, chan.at[my_y, 1]),
            )
        )
    ]

    def x_copy(index):
        cols = pl.ds(index * piece, piece)
        return pltpu.make_async_copy(x_hbm.at[:, cols], x_in.at[:, cols], x_sem.at[index])

    def proj_copies(layer, chunk, index=None):
        rows = pl.ds(chunk * CHUNK, CHUNK)
        cols = slice(None) if index is None else pl.ds(index * piece, piece)
        return [
            pltpu.make_async_copy(
                ref.at[layer, rows, cols],
                wp.at[layer, chunk, pl.ds(half * CHUNK, CHUNK), cols],
                wp_sem.at[layer, chunk, index or 0],
            )
            for half, ref in enumerate((wv_ref, wg_ref))
        ]

    def out_copy(layer):
        return pltpu.make_async_copy(ow_ref.at[layer], wo.at[layer], wo_sem.at[layer])

    smalls[0].start()
    for index in range(PIECES):
        x_copy(index).start()
        for copy in proj_copies(0, 0, index):
            copy.start()
    for copy in smalls[1:]:
        copy.start()
    for layer in range(LAYERS):
        for chunk in range(n_a):
            if layer or chunk:
                for copy in proj_copies(layer, chunk):
                    copy.start()
        out_copy(layer).start()

    barrier = pltpu.get_barrier_semaphore()
    for step in range(1, n_tp):
        pl.semaphore_signal(
            barrier, inc=1, device_id=tp_id(lax.rem(me + step, n_tp)), device_id_type=MESH
        )

    @pl.when(sp > 0)
    def _():
        pl.semaphore_signal(barrier, inc=1, device_id={"sp": sp - 1}, device_id_type=MESH)

    @pl.when(sp < n_sp - 1)
    def _():
        pl.semaphore_signal(barrier, inc=1, device_id={"sp": sp + 1}, device_id_type=MESH)

    part[...] = jnp.zeros(part.shape, jnp.float32)
    columns[...] = jnp.zeros(columns.shape, jnp.float32)

    pending = []

    def remote(source, target, send, recv, device):
        return pltpu.make_async_remote_copy(
            src_ref=source,
            dst_ref=target,
            send_sem=send,
            recv_sem=recv,
            device_id=tp_id(device),
            device_id_type=MESH,
        )

    def launch(copy):
        copy.start()
        pending.append(copy)

    def rows_of(span):
        return pl.ds(span[0], span[1] - span[0])

    def y_peer(step):
        return lax.rem(my_y + step, n_y)

    def y_origin(step):
        return lax.rem(my_y + n_y - step, n_y)

    def y_copy(phase, ref, step, chunk):
        target = y_peer(step) * CORES + core
        return remote(
            ref, ref, y_send.at[phase, step, chunk], y_recv.at[phase, step, chunk], target
        )

    def f_copy(phase, buf, step, chunk, owner, span):
        ref = buf.at[owner, chunk, rows_of(span)]
        return remote(
            ref, ref, f_send.at[phase, step, chunk], f_recv.at[phase, step, chunk], sibling
        )

    def chan_copy(step, slot):
        target = y_peer(step) * CORES + core
        return remote(chan.at[slot], chan.at[slot], chan_send.at[step], chan_recv.at[step], target)

    def prepare(index):
        gains = gain_ref[0:1, index * piece : (index + 1) * piece]

        @pl.loop(0, tokens // ROWS)
        def _(block):
            rows = pl.ds(pl.multiple_of(block * ROWS, ROWS), ROWS)
            squares = jnp.zeros((ROWS, LANES), jnp.float32)
            if index:
                squares = norm_squares[rows, :]
            for lane in range(piece // LANES):
                here = slice(index * piece + lane * LANES, index * piece + (lane + 1) * LANES)
                values = x_in[rows, here].astype(jnp.float32)
                squares = squares + values * values
                xg[rows, here] = (values * gains[:, lane * LANES : (lane + 1) * LANES]).astype(
                    jnp.bfloat16
                )
            norm_squares[rows, :] = squares

    def held(chunk):
        return slice(chunk * 2 * CHUNK, (chunk + 1) * 2 * CHUNK)

    def gate(chunk, first_row, count):
        rows = pl.ds(first_row, count)
        scaling = scale[rows, :]
        start = chunk * 2 * CHUNK
        pieces = []
        for lane in range(groups):
            at = start + lane * LANES
            value = accp[rows, at : at + LANES] * scaling
            gates = accp[rows, at + CHUNK : at + CHUNK + LANES] * scaling
            gated = (value * jax.nn.sigmoid(gates)).astype(jnp.bfloat16)
            ext[chunk * groups + lane, pl.ds(first_row + HALO, count), :] = gated.astype(
                jnp.float32
            )
            pieces.append(gated)
        return pieces

    def gate_rows(chunk, start, stop):
        @pl.loop(0, (stop - start) // HALO)
        def _(block):
            gate(chunk, pl.multiple_of(start + block * HALO, HALO), HALO)

    def halo_copy(layer, chunk):
        return pltpu.make_async_remote_copy(
            src_ref=halo_out.at[layer, chunk],
            dst_ref=halo_in.at[layer, chunk],
            send_sem=halo_send.at[layer, chunk],
            recv_sem=halo_recv.at[layer, chunk],
            device_id={"sp": lax.rem(sp + 1, n_sp)},
            device_id_type=MESH,
        )

    def send_halo(layer, chunk):
        for lane, gated in enumerate(gate(chunk, tokens - HALO, HALO)):
            halo_out[layer, chunk, :, lane * LANES : (lane + 1) * LANES] = gated

        @pl.when(sp < n_sp - 1)
        def _():
            halo_copy(layer, chunk).start()

    def receive_halo(layer, chunk):
        @pl.when(sp > 0)
        def _():
            halo_copy(layer, chunk).wait_recv()
            for lane in range(groups):
                ext[chunk * groups + lane, :HALO, :] = halo_in[
                    layer, chunk, :, lane * LANES : (lane + 1) * LANES
                ].astype(jnp.float32)

        @pl.when(sp == 0)
        def _():
            for lane in range(groups):
                ext[chunk * groups + lane, :HALO, :] = jnp.zeros((HALO, LANES), jnp.float32)

    def convolve(layer, half, chunk, start, stop):
        base = spans[layer][half][0]
        blocks = []
        while start < stop:
            count = min(ROWS, stop - start)
            blocks.append((start, count))
            start += count

        @pl.loop(chunk * groups, (chunk + 1) * groups)
        def _(lane):
            here = pl.ds(pl.multiple_of(lane * LANES, LANES), LANES)
            bias = bias_ref[layer : layer + 1, here]
            for first_row, count in blocks:
                tiles = count // SUBLANES
                sums = [jnp.broadcast_to(bias, (SUBLANES, LANES))] * tiles
                for residue in range(SUBLANES):
                    begin = first_row + HALO - K + 1 + residue
                    held_taps = range(residue, K, SUBLANES)
                    weights = [taps[layer, tap : tap + 1, here] for tap in held_taps]
                    for index in range(tiles + len(weights) - 1):
                        at = begin + index * SUBLANES
                        window = ext[lane, at : at + SUBLANES, :]
                        for step, weight in enumerate(weights):
                            tile = index - step
                            if 0 <= tile < tiles:
                                sums[tile] = sums[tile] + window * weight
                total = jnp.concatenate(sums, axis=0)
                filt[first_row : first_row + count, here] = total
                inner = slice(first_row - base, first_row - base + count)
                part[half, chunk, 0, inner, :] += total
                part[half, chunk, 1, inner, :] += total * total

    lane_index = lax.broadcasted_iota(jnp.int32, (HALO, LANES), 1)

    def centre(layer, half, chunk):
        start, stop = spans[layer][half]

        @pl.loop(0, (stop - start) // HALO)
        def _(block):
            inner = pl.ds(pl.multiple_of(block * HALO, HALO), HALO)
            rows = pl.ds(pl.multiple_of(start + block * HALO, HALO), HALO)
            mean = jnp.sum(part[half, chunk, 0, inner, :], axis=1, keepdims=True) / CHUNK
            squares = jnp.sum(part[half, chunk, 1, inner, :], axis=1, keepdims=True)
            for lane in range(groups):
                at = chunk * CHUNK + lane * LANES
                cf[layer, my_y, chunk, rows, lane * LANES : (lane + 1) * LANES] = (
                    filt[rows, at : at + LANES] - mean
                ).astype(jnp.bfloat16)
            packed = jnp.where(
                lane_index == chunk, mean, jnp.where(lane_index == n_a + chunk, squares, 0.0)
            )
            if chunk:
                packed = packed + columns[half, inner, :]
            columns[half, inner, :] = packed

    def send_centred(layer, half, phase, chunk):
        ref = cf.at[layer, my_y, chunk, rows_of(spans[layer][half])]
        for step in range(1, n_y):
            launch(y_copy(phase, ref, step, chunk))

    def stat_copy(layer, half, step, owner, target):
        ref = stat.at[layer, half, owner]
        index = layer * 2 + half
        return remote(ref, ref, stat_send.at[index, step], stat_recv.at[index, step], target)

    def send_stats(layer, half):
        stat[layer, half, me] = jnp.transpose(columns[half])[:SUBLANES]
        for step in range(1, n_tp):
            launch(stat_copy(layer, half, step, me, lax.rem(me + step, n_tp)))

    def to_columns(rows):
        fill = jnp.zeros((LANES - rows.shape[0], padded), jnp.float32)
        return jnp.transpose(jnp.concatenate((rows, fill), axis=0))

    def settle(layer, half):
        for step in range(1, n_tp):
            origin = lax.rem(me + n_tp - step, n_tp)
            stat_copy(layer, half, step, origin, origin).wait_recv()
        totals = jnp.sum(stat[layer, half], axis=0)
        mean_row = jnp.sum(totals[:n_a], axis=0, keepdims=True) * CHUNK / total_chans
        square_row = jnp.sum(totals[n_a : 2 * n_a], axis=0, keepdims=True) / total_chans
        rstd_row = lax.rsqrt(square_row - mean_row * mean_row + epsilon)
        rows = [rstd_row]
        for step in range(n_y):
            means = stat[layer, half, y_origin(step) * CORES + core]
            rows.append((means[:n_a] - mean_row) * rstd_row)
        columns[half] = to_columns(jnp.concatenate(rows, axis=0))

    def activate(layer, half, step, chunk):
        start, stop = spans[layer][half]
        origin = y_origin(step)
        owner = origin * CORES + core

        @pl.loop(0, (stop - start) // HALO)
        def _(block):
            inner = pl.ds(pl.multiple_of(block * HALO, HALO), HALO)
            rows = pl.ds(pl.multiple_of(start + block * HALO, HALO), HALO)
            at = 1 + step * n_a + chunk
            rstd = jnp.broadcast_to(columns[half, inner, 0:1], (HALO, LANES))
            shift = jnp.broadcast_to(columns[half, inner, at : at + 1], (HALO, LANES))
            for lane in range(groups):
                cols = slice(lane * LANES, (lane + 1) * LANES)
                here = slice(chunk * CHUNK + lane * LANES, chunk * CHUNK + (lane + 1) * LANES)
                values = cf[layer, origin, chunk, rows, cols].astype(jnp.float32) * rstd + shift
                values = (
                    values * chan[origin, 0, layer : layer + 1, here]
                    + chan[origin, 1, layer : layer + 1, here]
                )
                ag[layer, owner, chunk, rows, cols] = jax.nn.silu(values).astype(jnp.bfloat16)

    def own_activated(layer, half, phase):
        for chunk in range(n_a):
            activate(layer, half, 0, chunk)
            launch(f_copy(phase, ag.at[layer], 0, chunk, me, spans[layer][half]))

    def arrived_activated(layer, half, phase):
        for step in range(1, n_y):
            owner = y_origin(step) * CORES + core
            for chunk in range(n_a):
                ref = cf.at[layer, y_origin(step), chunk, rows_of(spans[layer][half])]
                y_copy(phase, ref, step, chunk).wait_recv()
                activate(layer, half, step, chunk)
                launch(f_copy(phase, ag.at[layer], step, chunk, owner, spans[layer][half]))

    def mix(layer, half, owner, first=False):
        rows = slice(*spans[layer][half])
        if not first:
            total = acco[rows, :]
        elif layer == 0:
            total = x_in[rows, pl.ds(pl.multiple_of(me * feats, LANES), feats)].astype(jnp.float32)
        else:
            total = res[rows, :]
        for chunk in range(n_a):
            start = pl.multiple_of(owner * chans + chunk * CHUNK, LANES)
            total = total + dot_nt(
                ag[layer, owner, chunk, rows, :], wo[layer, :, pl.ds(start, CHUNK)]
            )
        acco[rows, :] = total

    def mix_own(layer, half):
        mix(layer, half, me, True)

    def mix_arrived(layer, half):
        for step in range(1, n_y):
            mix(layer, half, y_origin(step) * CORES + core)

    def mix_sibling(layer, half, phase):
        for chunk in range(n_a):
            f_copy(phase, ag.at[layer], 0, chunk, sibling, spans[layer][half]).wait_recv()
        mix(layer, half, sibling)

    def mix_relayed(layer, half, phase):
        for step in range(1, n_y):
            owner = y_origin(step) * CORES + 1 - core
            for chunk in range(n_a):
                f_copy(phase, ag.at[layer], step, chunk, owner, spans[layer][half]).wait_recv()
            mix(layer, half, owner)

    def square_copy(half, step, owner, target):
        ref = square.at[half, owner]
        return remote(ref, ref, square_send.at[half, step], square_recv.at[half, step], target)

    def send_stream(half):
        span = spans[0][half]
        rows = slice(*span)
        squares = jnp.zeros((span[1] - span[0], LANES), jnp.float32)
        for chunk in range(n_f):
            first = pl.multiple_of(me * feats + chunk * CHUNK, LANES)
            gains = gain_ref[1:2, pl.ds(first, CHUNK)]
            for lane in range(groups):
                cols = slice(lane * LANES, (lane + 1) * LANES)
                here = slice(chunk * CHUNK + lane * LANES, chunk * CHUNK + (lane + 1) * LANES)
                rounded = acco[rows, here].astype(jnp.bfloat16).astype(jnp.float32)
                sg[me, chunk, rows, cols] = (rounded * gains[:, cols]).astype(jnp.bfloat16)
                res[rows, here] = rounded
                squares = squares + rounded * rounded
            ref = sg.at[me, chunk, rows_of(span)]
            for step in range(1, n_y):
                launch(y_copy(2 + half, ref, step, chunk))
            launch(f_copy(2 + half, sg, 0, chunk, me, span))
        norm_squares[rows, :] = squares

    def send_squares(half):
        span = spans[0][half]
        count = span[1] - span[0]
        squares = norm_squares[slice(*span), :]
        if count < padded:
            fill = jnp.zeros((padded - count, LANES), jnp.float32)
            squares = jnp.concatenate((squares, fill), axis=0)
        row = jnp.sum(jnp.transpose(squares), axis=0, keepdims=True)
        square[half, me] = jnp.broadcast_to(row, (SUBLANES, padded))
        for step in range(1, n_tp):
            launch(square_copy(half, step, me, lax.rem(me + step, n_tp)))

    def rescale(half):
        for step in range(1, n_tp):
            origin = lax.rem(me + n_tp - step, n_tp)
            square_copy(half, step, origin, origin).wait_recv()
        totals = jnp.sum(square[half], axis=0)[0:1] / width
        start, stop = spans[0][half]
        spread = jnp.transpose(
            jnp.broadcast_to(lax.rsqrt(totals + epsilon), (LANES, padded))
        )
        scale[start:stop, :] = spread[: stop - start]

    def project(half, owner, chunks, first):
        rows = slice(*spans[0][half])
        for block in range(n_a):
            total = None if first else accp[rows, held(block)]
            for chunk in chunks:
                start = pl.multiple_of(owner * feats + chunk * CHUNK, LANES)
                product = dot_nt(
                    sg[owner, chunk, rows, :], wp[1, block, :, pl.ds(start, CHUNK)]
                )
                total = product if total is None else total + product
            accp[rows, held(block)] = total

    def near_stream(half):
        project(half, me, range(n_f), True)
        for chunk in range(n_f):
            f_copy(2 + half, sg, 0, chunk, sibling, spans[0][half]).wait_recv()
        project(half, sibling, range(n_f), False)

    def arrive_stream(half, chunk):
        for step in range(1, n_y):
            origin = y_origin(step)
            owner = origin * CORES + core
            ref = sg.at[owner, chunk, rows_of(spans[0][half])]
            y_copy(2 + half, ref, step, chunk).wait_recv()
            launch(f_copy(2 + half, sg, step, chunk, owner, spans[0][half]))
            project(half, owner, (chunk,), False)

    def relayed_stream(half, chunk):
        for step in range(1, n_y):
            owner = y_origin(step) * CORES + 1 - core
            f_copy(2 + half, sg, step, chunk, owner, spans[0][half]).wait_recv()
            project(half, owner, (chunk,), False)

    def far_stream(half, chunks):
        for chunk in chunks:
            arrive_stream(half, chunk)
            if chunk:
                relayed_stream(half, chunk - 1)

    smalls[0].wait()
    for index in range(PIECES):
        cols = slice(index * piece, (index + 1) * piece)
        x_copy(index).wait()
        prepare(index)
        for copy in proj_copies(0, 0, index):
            copy.wait()
        product = dot_nt(xg[:, cols], wp[0, 0, :, cols])
        if index:
            accp[:, held(0)] += product
        else:
            accp[:, held(0)] = product

    @pl.loop(0, tokens // ROWS)
    def _(block):
        rows = pl.ds(pl.multiple_of(block * ROWS, ROWS), ROWS)
        scaling = lax.rsqrt(jnp.sum(norm_squares[rows, :], axis=1, keepdims=True) / width + epsilon)
        scale[rows, :] = jnp.broadcast_to(scaling, (ROWS, LANES))

    for copy in smalls[1:]:
        copy.wait()
    for layer in range(LAYERS):
        taps[layer] = raw_taps[:, layer, :]
    pl.semaphore_wait(
        barrier,
        n_tp - 1 + jnp.where(sp > 0, 1, 0) + jnp.where(sp < n_sp - 1, 1, 0),
    )
    for step in range(1, n_y):
        launch(chan_copy(step, my_y))

    for chunk in range(n_a):
        if chunk:
            for copy in proj_copies(0, chunk):
                copy.wait()
            accp[:, held(chunk)] = dot_nt(xg[...], wp[0, chunk])
        send_halo(0, chunk)
        gate_rows(chunk, 0, tokens - HALO)
        convolve(0, 0, chunk, *spans[0][0])
        centre(0, 0, chunk)
        send_centred(0, 0, 0, chunk)
    send_stats(0, 0)
    for chunk in range(n_a):
        convolve(0, 1, chunk, ROWS, spans[0][1][1])
        receive_halo(0, chunk)
        convolve(0, 1, chunk, 0, ROWS)
        centre(0, 1, chunk)
        send_centred(0, 1, 1, chunk)
    send_stats(0, 1)
    for step in range(1, n_y):
        chan_copy(step, y_origin(step)).wait_recv()
    settle(0, 0)
    own_activated(0, 0, 0)
    out_copy(0).wait()
    mix_own(0, 0)
    arrived_activated(0, 0, 0)
    mix_arrived(0, 0)
    mix_sibling(0, 0, 0)
    settle(0, 1)
    own_activated(0, 1, 1)
    mix_relayed(0, 0, 0)
    send_stream(0)
    send_squares(0)
    mix_own(0, 1)
    arrived_activated(0, 1, 1)
    mix_arrived(0, 1)
    mix_sibling(0, 1, 1)
    mix_relayed(0, 1, 1)
    send_stream(1)
    send_squares(1)
    part[...] = jnp.zeros(part.shape, jnp.float32)
    for chunk in range(n_a):
        for copy in proj_copies(1, chunk):
            copy.wait()
    near_stream(0)
    far_stream(0, range(n_f))
    near_stream(1)
    relayed_stream(0, n_f - 1)
    rescale(0)
    for chunk in range(n_a):
        send_halo(1, chunk)
        gate_rows(chunk, split, tokens - HALO)
        convolve(1, 0, chunk, *spans[1][0])
        centre(1, 0, chunk)
        send_centred(1, 0, 4, chunk)
    send_stats(1, 0)
    far_stream(1, range(n_f // 2))
    settle(1, 0)
    own_activated(1, 0, 4)
    far_stream(1, range(n_f // 2, n_f))
    relayed_stream(1, n_f - 1)
    rescale(1)
    for chunk in range(n_a):
        gate_rows(chunk, 0, split)
        convolve(1, 1, chunk, HALO, spans[1][1][1])
        receive_halo(1, chunk)
        convolve(1, 1, chunk, 0, HALO)
        centre(1, 1, chunk)
        send_centred(1, 1, 5, chunk)
    send_stats(1, 1)
    out_copy(1).wait()
    mix_own(1, 0)
    mix_sibling(1, 0, 4)
    arrived_activated(1, 0, 4)
    mix_arrived(1, 0)
    settle(1, 1)
    own_activated(1, 1, 5)
    mix_own(1, 1)
    mix_relayed(1, 0, 4)
    mix_sibling(1, 1, 5)
    arrived_activated(1, 1, 5)
    mix_arrived(1, 1)
    mix_relayed(1, 1, 5)
    out_ref[...] = acco[...].astype(jnp.bfloat16)

    @pl.when(sp < n_sp - 1)
    def _():
        for layer in range(LAYERS):
            for chunk in range(n_a):
                halo_copy(layer, chunk).wait_send()

    for copy in pending:
        copy.wait_send()


def fused(mesh, stream, norm_gain, value_weight, gate_weight, conv_kernel, conv_bias,
          channel_gain, channel_bias, out_weight):
    n_tp, n_sp = mesh.shape["tp"], mesh.shape["sp"]
    width, tokens = stream.shape
    chans, feats = value_weight.shape[1], out_weight.shape[1]
    split = (tokens // 2 - HALO) // HALO * HALO
    n_y = n_tp // CORES
    n_a, n_f = chans // CHUNK, feats // CHUNK
    fits = (
        n_tp % CORES == 0
        and chans % CHUNK == 0
        and feats % CHUNK == 0
        and width % (PIECES * CHUNK) == 0
        and tokens % ROWS == 0
        and split % ROWS == 0
        and tokens >= 4 * ROWS
        and LAYERS == 2
        and n_tp <= 8
        and 2 * n_a <= SUBLANES
        and 1 + n_y * n_a <= LANES
    )
    if not fits:
        return local(stream, norm_gain, value_weight, gate_weight, conv_kernel, conv_bias,
                     channel_gain, channel_bias, out_weight)
    padded = -(-(tokens - split) // LANES) * LANES
    most = max(n_a, n_f)
    f32, bf16 = jnp.float32, jnp.bfloat16
    dma = pltpu.SemaphoreType.DMA
    out = pl.pallas_call(
        functools.partial(kernel, n_tp, n_sp, split),
        out_shape=jax.ShapeDtypeStruct((tokens, feats), bf16),
        in_specs=[pl.BlockSpec(memory_space=pl.ANY)] * 9,
        out_specs=pl.BlockSpec(memory_space=pltpu.VMEM),
        scratch_shapes=[
            pltpu.VMEM((LAYERS, width), f32),
            pltpu.VMEM((K, LAYERS, chans), f32),
            pltpu.VMEM((LAYERS, chans), f32),
            pltpu.VMEM((n_y, 2, LAYERS, chans), f32),
            pltpu.VMEM((LAYERS, n_a, 2 * CHUNK, width), bf16),
            pltpu.VMEM((LAYERS, feats, chans * n_tp), bf16),
            pltpu.VMEM((tokens, width), bf16),
            pltpu.VMEM((tokens, width), bf16),
            pltpu.VMEM((chans // LANES, HALO + tokens, LANES), f32),
            pltpu.VMEM((tokens, chans), f32),
            pltpu.VMEM((LAYERS, K, chans), f32),
            pltpu.VMEM((tokens, LANES), f32),
            pltpu.VMEM((tokens, LANES), f32),
            pltpu.VMEM((2, n_a, 2, padded, LANES), f32),
            pltpu.VMEM((2, padded, LANES), f32),
            pltpu.VMEM((LAYERS, n_a, HALO, CHUNK), bf16),
            pltpu.VMEM((LAYERS, n_a, HALO, CHUNK), bf16),
            pltpu.VMEM((LAYERS, 2, n_tp, SUBLANES, padded), f32),
            pltpu.VMEM((2, n_tp, SUBLANES, padded), f32),
            pltpu.VMEM((LAYERS, n_y, n_a, tokens, CHUNK), bf16),
            pltpu.VMEM((LAYERS, n_tp, n_a, tokens, CHUNK), bf16),
            pltpu.VMEM((n_tp, n_f, tokens, CHUNK), bf16),
            pltpu.VMEM((tokens, 2 * chans), f32),
            pltpu.VMEM((tokens, feats), f32),
            pltpu.VMEM((tokens, feats), f32),
            dma((5,)),
            dma((PIECES,)),
            dma((LAYERS, n_a, PIECES)),
            dma((LAYERS,)),
            dma((n_y,)),
            dma((n_y,)),
            dma((LAYERS, n_a)),
            dma((LAYERS, n_a)),
            dma((LAYERS * 2, n_tp)),
            dma((LAYERS * 2, n_tp)),
            dma((2, n_tp)),
            dma((2, n_tp)),
            dma((6, n_y, most)),
            dma((6, n_y, most)),
            dma((6, n_y, most)),
            dma((6, n_y, most)),
        ],
        compiler_params=pltpu.CompilerParams(
            collective_id=0, has_side_effects=True, vmem_limit_bytes=60 * 1024 * 1024
        ),
    )(stream.T, norm_gain, jnp.transpose(conv_kernel, (2, 0, 1)), conv_bias, channel_gain, channel_bias,
       value_weight, gate_weight, out_weight)
    return out.T


def solution(mesh):
    placed = (
        P(None, ("grp", "sp")),
        P(),
        P(None, "tp", None),
        P(None, "tp", None),
        P(None, "tp", None),
        P(None, "tp"),
        P(None, "tp"),
        P(None, "tp"),
        P(None, "tp", None),
    )
    return jax.shard_map(
        functools.partial(fused, mesh), mesh=mesh, in_specs=placed, out_specs=P("tp", ("grp", "sp")), check_vma=False
    )
```

time: 57.5 us -> 64.9 us (1.13)
  Pallas kernels: 55 us -> 62.8 us
    pallas_call x1, Pallas kernels: 55 us -> 62.8 us  [fused(): pl.pallas_call(functools.partial(kernel, n_tp, n_sp, split), out_shape=ja...]
where the time goes in v1:
time: 64.9 us; the launch traced here: 64.7 us
  Pallas kernels  62.8 us (97%)
  local copies, waits for them, and re-layouts  1.97 us (3%)
    pallas_call x1, Pallas kernels, fused(): pl.pallas_call(functools.partial(kernel, n_tp, n_sp, split), out_shape=ja...  62.8 us
    unnamed x1, local copies, waits for them, and re-layouts  1.97 us

profile of v1, /device:TPU:0, one launch (start us, length us, event | category | flops | bytes accessed | tf_op | source)
XLA Modules:
  0.0 64.7 jit_solution(10859531461044683329)
XLA Ops:
  0.0 62.8 %shard_map.91 = bf16[320,1024]{1,0:T(8,128)(2,1)} custom-call(bf16[320,4096]{1,0:T(8,128)(2,1)} %bitcast.3, f32[2,4096]{1,0:T(2,128)} %gain_hbm.1, f32[31,2,512]{2,1,0:T(2,128)} %bitcast.5, f32[2,512]{1,0:T(2,128)} %bias_hbm.1, f32[2,512]{1,0:T(2,128)} %chan_gain_hbm.1, f32[2,512]{1,0:T(2,128)} %chan_bias_hbm.1, bf16[2,512,4096]{2,1,0:T(8,128)(2,1)} %wv_ref.1, ...), custom_call_target="tpu_custom_call" | custom-call | tf_op jit(solution)/shard_map/pallas_call | solution.py:769
  62.8 2.0 %copy.11 = bf16[1024,320]{0,1:T(8,128)(2,1)} copy(bf16[1024,320]{0,1:T(8,128)(2,1)} %bitcast.4) | data formatting | bytes 1310720

commit v2 on v1

--- a/solution.py
+++ b/solution.py
@@ -231,12 +231,6 @@
             copy.start()
     for copy in smalls[1:]:
         copy.start()
-    for layer in range(LAYERS):
-        for chunk in range(n_a):
-            if layer or chunk:
-                for copy in proj_copies(layer, chunk):
-                    copy.start()
-        out_copy(layer).start()
 
     barrier = pltpu.get_barrier_semaphore()
     for step in range(1, n_tp):
@@ -319,14 +313,14 @@
 
     def gate(chunk, first_row, count):
         rows = pl.ds(first_row, count)
-        scaling = scale[rows, :]
+        halved = scale[rows, :]
         start = chunk * 2 * CHUNK
         pieces = []
         for lane in range(groups):
             at = start + lane * LANES
-            value = accp[rows, at : at + LANES] * scaling
-            gates = accp[rows, at + CHUNK : at + CHUNK + LANES] * scaling
-            gated = (value * jax.nn.sigmoid(gates)).astype(jnp.bfloat16)
+            value = accp[rows, at : at + LANES] * halved
+            gates = accp[rows, at + CHUNK : at + CHUNK + LANES] * halved
+            gated = (value + value * jnp.tanh(gates)).astype(jnp.bfloat16)
             ext[chunk * groups + lane, pl.ds(first_row + HALO, count), :] = gated.astype(
                 jnp.float32
             )
@@ -407,10 +401,9 @@
     def centre(layer, half, chunk):
         start, stop = spans[layer][half]
 
-        @pl.loop(0, (stop - start) // HALO)
-        def _(block):
-            inner = pl.ds(pl.multiple_of(block * HALO, HALO), HALO)
-            rows = pl.ds(pl.multiple_of(start + block * HALO, HALO), HALO)
+        for block in range((stop - start) // HALO):
+            inner = slice(block * HALO, (block + 1) * HALO)
+            rows = slice(start + block * HALO, start + (block + 1) * HALO)
             mean = jnp.sum(part[half, chunk, 0, inner, :], axis=1, keepdims=True) / CHUNK
             squares = jnp.sum(part[half, chunk, 1, inner, :], axis=1, keepdims=True)
             for lane in range(groups):
@@ -463,22 +456,21 @@
         origin = y_origin(step)
         owner = origin * CORES + core
 
-        @pl.loop(0, (stop - start) // HALO)
-        def _(block):
-            inner = pl.ds(pl.multiple_of(block * HALO, HALO), HALO)
-            rows = pl.ds(pl.multiple_of(start + block * HALO, HALO), HALO)
-            at = 1 + step * n_a + chunk
+        at = 1 + step * n_a + chunk
+        gains = 0.5 * chan[origin, 0, layer : layer + 1, chunk * CHUNK : (chunk + 1) * CHUNK]
+        biases = 0.5 * chan[origin, 1, layer : layer + 1, chunk * CHUNK : (chunk + 1) * CHUNK]
+        for block in range((stop - start) // HALO):
+            inner = slice(block * HALO, (block + 1) * HALO)
+            rows = slice(start + block * HALO, start + (block + 1) * HALO)
             rstd = jnp.broadcast_to(columns[half, inner, 0:1], (HALO, LANES))
             shift = jnp.broadcast_to(columns[half, inner, at : at + 1], (HALO, LANES))
             for lane in range(groups):
                 cols = slice(lane * LANES, (lane + 1) * LANES)
-                here = slice(chunk * CHUNK + lane * LANES, chunk * CHUNK + (lane + 1) * LANES)
                 values = cf[layer, origin, chunk, rows, cols].astype(jnp.float32) * rstd + shift
-                values = (
-                    values * chan[origin, 0, layer : layer + 1, here]
-                    + chan[origin, 1, layer : layer + 1, here]
+                values = values * gains[:, cols] + biases[:, cols]
+                ag[layer, owner, chunk, rows, cols] = (values + values * jnp.tanh(values)).astype(
+                    jnp.bfloat16
                 )
-                ag[layer, owner, chunk, rows, cols] = jax.nn.silu(values).astype(jnp.bfloat16)
 
     def own_activated(layer, half, phase):
         for chunk in range(n_a):
@@ -494,7 +486,7 @@
                 activate(layer, half, step, chunk)
                 launch(f_copy(phase, ag.at[layer], step, chunk, owner, spans[layer][half]))
 
-    def mix(layer, half, owner, first=False):
+    def mix(layer, half, owner, chunks, first=False, last=False):
         rows = slice(*spans[layer][half])
         if not first:
             total = acco[rows, :]
@@ -502,31 +494,36 @@
             total = x_in[rows, pl.ds(pl.multiple_of(me * feats, LANES), feats)].astype(jnp.float32)
         else:
             total = res[rows, :]
-        for chunk in range(n_a):
+        for chunk in chunks:
             start = pl.multiple_of(owner * chans + chunk * CHUNK, LANES)
             total = total + dot_nt(
                 ag[layer, owner, chunk, rows, :], wo[layer, :, pl.ds(start, CHUNK)]
             )
-        acco[rows, :] = total
+        if last:
+            out_ref[rows, :] = total.astype(jnp.bfloat16)
+        else:
+            acco[rows, :] = total
 
     def mix_own(layer, half):
-        mix(layer, half, me, True)
+        mix(layer, half, me, range(n_a), True)
 
     def mix_arrived(layer, half):
         for step in range(1, n_y):
-            mix(layer, half, y_origin(step) * CORES + core)
+            mix(layer, half, y_origin(step) * CORES + core, range(n_a))
 
     def mix_sibling(layer, half, phase):
         for chunk in range(n_a):
             f_copy(phase, ag.at[layer], 0, chunk, sibling, spans[layer][half]).wait_recv()
-        mix(layer, half, sibling)
-
-    def mix_relayed(layer, half, phase):
+        mix(layer, half, sibling, range(n_a))
+
+    def mix_relayed(layer, half, phase, groups_of):
         for step in range(1, n_y):
             owner = y_origin(step) * CORES + 1 - core
-            for chunk in range(n_a):
-                f_copy(phase, ag.at[layer], step, chunk, owner, spans[layer][half]).wait_recv()
-            mix(layer, half, owner)
+            for chunks in groups_of:
+                for chunk in chunks:
+                    f_copy(phase, ag.at[layer], step, chunk, owner, spans[layer][half]).wait_recv()
+                final = step == n_y - 1 and chunks[-1] == n_a - 1
+                mix(layer, half, owner, chunks, False, layer == LAYERS - 1 and final)
 
     def square_copy(half, step, owner, target):
         ref = square.at[half, owner]
@@ -546,16 +543,16 @@
                 sg[me, chunk, rows, cols] = (rounded * gains[:, cols]).astype(jnp.bfloat16)
                 res[rows, here] = rounded
                 squares = squares + rounded * rounded
+            if chunk == n_f - 1:
+                send_squares(half, squares)
             ref = sg.at[me, chunk, rows_of(span)]
             for step in range(1, n_y):
                 launch(y_copy(2 + half, ref, step, chunk))
             launch(f_copy(2 + half, sg, 0, chunk, me, span))
-        norm_squares[rows, :] = squares
-
-    def send_squares(half):
+
+    def send_squares(half, squares):
         span = spans[0][half]
         count = span[1] - span[0]
-        squares = norm_squares[slice(*span), :]
         if count < padded:
             fill = jnp.zeros((padded - count, LANES), jnp.float32)
             squares = jnp.concatenate((squares, fill), axis=0)
@@ -571,7 +568,7 @@
         totals = jnp.sum(square[half], axis=0)[0:1] / width
         start, stop = spans[0][half]
         spread = jnp.transpose(
-            jnp.broadcast_to(lax.rsqrt(totals + epsilon), (LANES, padded))
+            jnp.broadcast_to(0.5 * lax.rsqrt(totals + epsilon), (LANES, padded))
         )
         scale[start:stop, :] = spread[: stop - start]
 
@@ -614,6 +611,7 @@
             if chunk:
                 relayed_stream(half, chunk - 1)
 
+    everything = range(n_a)
     smalls[0].wait()
     for index in range(PIECES):
         cols = slice(index * piece, (index + 1) * piece)
@@ -621,6 +619,10 @@
         prepare(index)
         for copy in proj_copies(0, 0, index):
             copy.wait()
+        if index == PIECES - 1:
+            for chunk in range(1, n_a):
+                for copy in proj_copies(0, chunk):
+                    copy.start()
         product = dot_nt(xg[:, cols], wp[0, 0, :, cols])
         if index:
             accp[:, held(0)] += product
@@ -631,7 +633,7 @@
     def _(block):
         rows = pl.ds(pl.multiple_of(block * ROWS, ROWS), ROWS)
         scaling = lax.rsqrt(jnp.sum(norm_squares[rows, :], axis=1, keepdims=True) / width + epsilon)
-        scale[rows, :] = jnp.broadcast_to(scaling, (ROWS, LANES))
+        scale[rows, :] = jnp.broadcast_to(0.5 * scaling, (ROWS, LANES))
 
     for copy in smalls[1:]:
         copy.wait()
@@ -653,15 +655,22 @@
         gate_rows(chunk, 0, tokens - HALO)
         convolve(0, 0, chunk, *spans[0][0])
         centre(0, 0, chunk)
+        if chunk == n_a - 1:
+            send_stats(0, 0)
         send_centred(0, 0, 0, chunk)
-    send_stats(0, 0)
+    out_copy(0).start()
     for chunk in range(n_a):
         convolve(0, 1, chunk, ROWS, spans[0][1][1])
         receive_halo(0, chunk)
         convolve(0, 1, chunk, 0, ROWS)
         centre(0, 1, chunk)
+        if chunk == n_a - 1:
+            send_stats(0, 1)
         send_centred(0, 1, 1, chunk)
-    send_stats(0, 1)
+    for chunk in range(n_a):
+        for copy in proj_copies(1, chunk):
+            copy.start()
+    out_copy(1).start()
     for step in range(1, n_y):
         chan_copy(step, y_origin(step)).wait_recv()
     settle(0, 0)
@@ -673,16 +682,14 @@
     mix_sibling(0, 0, 0)
     settle(0, 1)
     own_activated(0, 1, 1)
-    mix_relayed(0, 0, 0)
+    mix_relayed(0, 0, 0, [everything])
     send_stream(0)
-    send_squares(0)
     mix_own(0, 1)
     arrived_activated(0, 1, 1)
     mix_arrived(0, 1)
     mix_sibling(0, 1, 1)
-    mix_relayed(0, 1, 1)
+    mix_relayed(0, 1, 1, [everything])
     send_stream(1)
-    send_squares(1)
     part[...] = jnp.zeros(part.shape, jnp.float32)
     for chunk in range(n_a):
         for copy in proj_copies(1, chunk):
@@ -697,8 +704,9 @@
         gate_rows(chunk, split, tokens - HALO)
         convolve(1, 0, chunk, *spans[1][0])
         centre(1, 0, chunk)
+    send_stats(1, 0)
+    for chunk in range(n_a):
         send_centred(1, 0, 4, chunk)
-    send_stats(1, 0)
     far_stream(1, range(n_f // 2))
     settle(1, 0)
     own_activated(1, 0, 4)
@@ -711,8 +719,9 @@
         receive_halo(1, chunk)
         convolve(1, 1, chunk, 0, HALO)
         centre(1, 1, chunk)
+        if chunk == n_a - 1:
+            send_stats(1, 1)
         send_centred(1, 1, 5, chunk)
-    send_stats(1, 1)
     out_copy(1).wait()
     mix_own(1, 0)
     mix_sibling(1, 0, 4)
@@ -721,12 +730,11 @@
     settle(1, 1)
     own_activated(1, 1, 5)
     mix_own(1, 1)
-    mix_relayed(1, 0, 4)
+    mix_relayed(1, 0, 4, [everything])
     mix_sibling(1, 1, 5)
     arrived_activated(1, 1, 5)
     mix_arrived(1, 1)
-    mix_relayed(1, 1, 5)
-    out_ref[...] = acco[...].astype(jnp.bfloat16)
+    mix_relayed(1, 1, 5, [(chunk,) for chunk in everything])
 
     @pl.when(sp < n_sp - 1)
     def _():
@@ -815,10 +823,15 @@
             dma((6, n_y, most)),
         ],
         compiler_params=pltpu.CompilerParams(
-            collective_id=0, has_side_effects=True, vmem_limit_bytes=60 * 1024 * 1024
+            collective_id=0, has_side_effects=True, vmem_limit_bytes=50 * 1024 * 1024
         ),
-    )(stream.T, norm_gain, jnp.transpose(conv_kernel, (2, 0, 1)), conv_bias, channel_gain, channel_bias,
-       value_weight, gate_weight, out_weight)
+    )(*(
+        pltpu.with_memory_space_constraint(value, pltpu.HBM)
+        for value in (
+            stream.T, norm_gain, jnp.transpose(conv_kernel, (2, 0, 1)), conv_bias, channel_gain,
+            channel_bias, value_weight, gate_weight, out_weight,
+        )
+    ))
     return out.T
 
 

time: 64.9 us -> 49.9 us (0.77)
  Pallas kernels: 62.8 us -> 48.9 us
  local copies, waits for them, and re-layouts: 1.97 us -> 0.84 us
    pallas_call x1, Pallas kernels: 62.8 us -> 48.9 us  [fused(): pl.pallas_call(functools.partial(kernel, n_tp, n_sp, split), out_shape=ja...]
    unnamed x1, local copies, waits for them, and re-layouts: 1.97 us -> 0.84 us
where the time goes in v2:
time: 49.9 us; the launch traced here: 49.8 us
  Pallas kernels  48.9 us (98%)
  local copies, waits for them, and re-layouts  0.84 us (2%)
    pallas_call x1, Pallas kernels, fused(): pl.pallas_call(functools.partial(kernel, n_tp, n_sp, split), out_shape=ja...  48.9 us

profile of v2, /device:TPU:0, one launch (start us, length us, event | category | flops | bytes accessed | tf_op | source)
XLA Modules:
  0.0 49.8 jit_solution(4909957345039294166)
XLA Ops:
  0.0 48.9 %shard_map.91 = bf16[320,1024]{1,0:T(8,128)(2,1)S(1)} custom-call(bf16[320,4096]{1,0:T(8,128)(2,1)} %bitcast.4, f32[2,4096]{1,0:T(2,128)} %gain_hbm.1, f32[31,2,512]{2,1,0:T(2,128)} %bitcast.5, f32[2,512]{1,0:T(2,128)} %bias_hbm.1, f32[2,512]{1,0:T(2,128)} %chan_gain_hbm.1, f32[2,512]{1,0:T(2,128)} %chan_bias_hbm.1, bf16[2,512,4096]{2,1,0:T(8,128)(2,1)} %wv_ref.1, ...), custom_call_target="tpu_custom_call" | custom-call | tf_op jit(solution)/shard_map/pallas_call | solution.py:777
  48.9 0.8 %copy.11 = bf16[1024,320]{0,1:T(8,128)(2,1)} copy(bf16[1024,320]{0,1:T(8,128)(2,1)S(1)} %bitcast.3) | data formatting | bytes 1310720

commit v3 on v2

--- a/solution.py
+++ b/solution.py
@@ -224,13 +224,12 @@
     def out_copy(layer):
         return pltpu.make_async_copy(ow_ref.at[layer], wo.at[layer], wo_sem.at[layer])
 
-    smalls[0].start()
+    for copy in smalls:
+        copy.start()
     for index in range(PIECES):
         x_copy(index).start()
         for copy in proj_copies(0, 0, index):
             copy.start()
-    for copy in smalls[1:]:
-        copy.start()
 
     barrier = pltpu.get_barrier_semaphore()
     for step in range(1, n_tp):
@@ -265,6 +264,10 @@
         copy.start()
         pending.append(copy)
 
+    def drain(keep=0):
+        while len(pending) > keep:
+            pending.pop(0).wait_send()
+
     def rows_of(span):
         return pl.ds(span[0], span[1] - span[0])
 
@@ -292,17 +295,13 @@
 
     def prepare(index):
         gains = gain_ref[0:1, index * piece : (index + 1) * piece]
-
-        @pl.loop(0, tokens // ROWS)
-        def _(block):
-            rows = pl.ds(pl.multiple_of(block * ROWS, ROWS), ROWS)
-            squares = jnp.zeros((ROWS, LANES), jnp.float32)
-            if index:
-                squares = norm_squares[rows, :]
+        for first_row in range(0, tokens, ROWS):
+            rows = slice(first_row, first_row + ROWS)
+            squares = norm_squares[rows, :] if index else None
             for lane in range(piece // LANES):
                 here = slice(index * piece + lane * LANES, index * piece + (lane + 1) * LANES)
                 values = x_in[rows, here].astype(jnp.float32)
-                squares = squares + values * values
+                squares = values * values if squares is None else squares + values * values
                 xg[rows, here] = (values * gains[:, lane * LANES : (lane + 1) * LANES]).astype(
                     jnp.bfloat16
                 )
@@ -477,16 +476,19 @@
             activate(layer, half, 0, chunk)
             launch(f_copy(phase, ag.at[layer], 0, chunk, me, spans[layer][half]))
 
-    def arrived_activated(layer, half, phase):
+    def arrive(layer, half, phase, chunk):
         for step in range(1, n_y):
             owner = y_origin(step) * CORES + core
-            for chunk in range(n_a):
-                ref = cf.at[layer, y_origin(step), chunk, rows_of(spans[layer][half])]
-                y_copy(phase, ref, step, chunk).wait_recv()
-                activate(layer, half, step, chunk)
-                launch(f_copy(phase, ag.at[layer], step, chunk, owner, spans[layer][half]))
-
-    def mix(layer, half, owner, chunks, first=False, last=False):
+            ref = cf.at[layer, y_origin(step), chunk, rows_of(spans[layer][half])]
+            y_copy(phase, ref, step, chunk).wait_recv()
+            activate(layer, half, step, chunk)
+            launch(f_copy(phase, ag.at[layer], step, chunk, owner, spans[layer][half]))
+
+    def from_sibling(layer, half, phase, chunk, step=0):
+        owner = y_origin(step) * CORES + 1 - core
+        f_copy(phase, ag.at[layer], step, chunk, owner, spans[layer][half]).wait_recv()
+
+    def mix(layer, half, parts, first=False, last=False):
         rows = slice(*spans[layer][half])
         if not first:
             total = acco[rows, :]
@@ -494,7 +496,7 @@
             total = x_in[rows, pl.ds(pl.multiple_of(me * feats, LANES), feats)].astype(jnp.float32)
         else:
             total = res[rows, :]
-        for chunk in chunks:
+        for owner, chunk in parts:
             start = pl.multiple_of(owner * chans + chunk * CHUNK, LANES)
             total = total + dot_nt(
                 ag[layer, owner, chunk, rows, :], wo[layer, :, pl.ds(start, CHUNK)]
@@ -504,26 +506,39 @@
         else:
             acco[rows, :] = total
 
-    def mix_own(layer, half):
-        mix(layer, half, me, range(n_a), True)
-
-    def mix_arrived(layer, half):
-        for step in range(1, n_y):
-            mix(layer, half, y_origin(step) * CORES + core, range(n_a))
-
-    def mix_sibling(layer, half, phase):
-        for chunk in range(n_a):
-            f_copy(phase, ag.at[layer], 0, chunk, sibling, spans[layer][half]).wait_recv()
-        mix(layer, half, sibling, range(n_a))
-
-    def mix_relayed(layer, half, phase, groups_of):
-        for step in range(1, n_y):
-            owner = y_origin(step) * CORES + 1 - core
-            for chunks in groups_of:
-                for chunk in chunks:
-                    f_copy(phase, ag.at[layer], step, chunk, owner, spans[layer][half]).wait_recv()
-                final = step == n_y - 1 and chunks[-1] == n_a - 1
-                mix(layer, half, owner, chunks, False, layer == LAYERS - 1 and final)
+    everything = range(n_a)
+    others = range(1, n_y)
+
+    def own(chunks):
+        return [(me, chunk) for chunk in chunks]
+
+    def next_door(chunks):
+        return [(sibling, chunk) for chunk in chunks]
+
+    def across(chunks):
+        return [(y_origin(step) * CORES + core, chunk) for step in others for chunk in chunks]
+
+    def relayed(chunks):
+        return [(y_origin(step) * CORES + 1 - core, chunk) for step in others for chunk in chunks]
+
+    def branch(layer, half, phase, ahead=None):
+        own_activated(layer, half, phase)
+        mix(layer, half, own(everything), True)
+        for chunk in everything[:-1]:
+            arrive(layer, half, phase, chunk)
+        for chunk in everything:
+            from_sibling(layer, half, phase, chunk)
+        mix(layer, half, next_door(everything) + across(everything[:-1]))
+        if ahead is not None:
+            ahead()
+        arrive(layer, half, phase, n_a - 1)
+        for step in others:
+            for chunk in everything[:-1]:
+                from_sibling(layer, half, phase, chunk, step)
+        mix(layer, half, across(everything[-1:]) + relayed(everything[:-1]))
+        for step in others:
+            from_sibling(layer, half, phase, n_a - 1, step)
+        mix(layer, half, relayed(everything[-1:]), False, layer == LAYERS - 1)
 
     def square_copy(half, step, owner, target):
         ref = square.at[half, owner]
@@ -584,8 +599,10 @@
                 total = product if total is None else total + product
             accp[rows, held(block)] = total
 
-    def near_stream(half):
+    def own_stream(half):
         project(half, me, range(n_f), True)
+
+    def sibling_stream(half):
         for chunk in range(n_f):
             f_copy(2 + half, sg, 0, chunk, sibling, spans[0][half]).wait_recv()
         project(half, sibling, range(n_f), False)
@@ -605,48 +622,41 @@
             f_copy(2 + half, sg, step, chunk, owner, spans[0][half]).wait_recv()
             project(half, owner, (chunk,), False)
 
-    def far_stream(half, chunks):
-        for chunk in chunks:
-            arrive_stream(half, chunk)
-            if chunk:
-                relayed_stream(half, chunk - 1)
-
-    everything = range(n_a)
-    smalls[0].wait()
+    for copy in smalls:
+        copy.wait()
+    for layer in range(LAYERS):
+        taps[layer] = raw_taps[:, layer, :]
+    x_copy(0).wait()
+    prepare(0)
     for index in range(PIECES):
         cols = slice(index * piece, (index + 1) * piece)
-        x_copy(index).wait()
-        prepare(index)
         for copy in proj_copies(0, 0, index):
             copy.wait()
-        if index == PIECES - 1:
+        if index < PIECES - 1:
+            x_copy(index + 1).wait()
+        if index == PIECES // 2:
             for chunk in range(1, n_a):
                 for copy in proj_copies(0, chunk):
                     copy.start()
         product = dot_nt(xg[:, cols], wp[0, 0, :, cols])
+        if index < PIECES - 1:
+            prepare(index + 1)
         if index:
             accp[:, held(0)] += product
         else:
             accp[:, held(0)] = product
 
-    @pl.loop(0, tokens // ROWS)
-    def _(block):
-        rows = pl.ds(pl.multiple_of(block * ROWS, ROWS), ROWS)
+    for first_row in range(0, tokens, ROWS):
+        rows = slice(first_row, first_row + ROWS)
         scaling = lax.rsqrt(jnp.sum(norm_squares[rows, :], axis=1, keepdims=True) / width + epsilon)
         scale[rows, :] = jnp.broadcast_to(0.5 * scaling, (ROWS, LANES))
 
-    for copy in smalls[1:]:
-        copy.wait()
-    for layer in range(LAYERS):
-        taps[layer] = raw_taps[:, layer, :]
     pl.semaphore_wait(
         barrier,
         n_tp - 1 + jnp.where(sp > 0, 1, 0) + jnp.where(sp < n_sp - 1, 1, 0),
     )
-    for step in range(1, n_y):
-        launch(chan_copy(step, my_y))
-
-    for chunk in range(n_a):
+
+    for chunk in everything:
         if chunk:
             for copy in proj_copies(0, chunk):
                 copy.wait()
@@ -658,8 +668,11 @@
         if chunk == n_a - 1:
             send_stats(0, 0)
         send_centred(0, 0, 0, chunk)
+        if chunk == 0:
+            for step in others:
+                launch(chan_copy(step, my_y))
     out_copy(0).start()
-    for chunk in range(n_a):
+    for chunk in everything:
         convolve(0, 1, chunk, ROWS, spans[0][1][1])
         receive_halo(0, chunk)
         convolve(0, 1, chunk, 0, ROWS)
@@ -667,53 +680,54 @@
         if chunk == n_a - 1:
             send_stats(0, 1)
         send_centred(0, 1, 1, chunk)
-    for chunk in range(n_a):
+    for chunk in everything:
         for copy in proj_copies(1, chunk):
             copy.start()
     out_copy(1).start()
-    for step in range(1, n_y):
+    for step in others:
         chan_copy(step, y_origin(step)).wait_recv()
+    out_copy(0).wait()
     settle(0, 0)
-    own_activated(0, 0, 0)
-    out_copy(0).wait()
-    mix_own(0, 0)
-    arrived_activated(0, 0, 0)
-    mix_arrived(0, 0)
-    mix_sibling(0, 0, 0)
+    branch(0, 0, 0)
+    send_stream(0)
     settle(0, 1)
-    own_activated(0, 1, 1)
-    mix_relayed(0, 0, 0, [everything])
-    send_stream(0)
-    mix_own(0, 1)
-    arrived_activated(0, 1, 1)
-    mix_arrived(0, 1)
-    mix_sibling(0, 1, 1)
-    mix_relayed(0, 1, 1, [everything])
+    branch(0, 1, 1)
+    settled = len(pending)
     send_stream(1)
     part[...] = jnp.zeros(part.shape, jnp.float32)
-    for chunk in range(n_a):
+    for chunk in everything:
         for copy in proj_copies(1, chunk):
             copy.wait()
-    near_stream(0)
-    far_stream(0, range(n_f))
-    near_stream(1)
+    own_stream(0)
+    sibling_stream(0)
+    for chunk in range(n_f):
+        if chunk == 1:
+            own_stream(1)
+        if chunk == 2:
+            sibling_stream(1)
+        if chunk == n_f - 1:
+            drain(len(pending) - settled)
+        arrive_stream(0, chunk)
+        if chunk:
+            relayed_stream(0, chunk - 1)
     relayed_stream(0, n_f - 1)
     rescale(0)
-    for chunk in range(n_a):
+    for chunk in everything:
         send_halo(1, chunk)
         gate_rows(chunk, split, tokens - HALO)
         convolve(1, 0, chunk, *spans[1][0])
         centre(1, 0, chunk)
+    streamed = len(pending)
     send_stats(1, 0)
-    for chunk in range(n_a):
+    for chunk in everything:
         send_centred(1, 0, 4, chunk)
-    far_stream(1, range(n_f // 2))
-    settle(1, 0)
-    own_activated(1, 0, 4)
-    far_stream(1, range(n_f // 2, n_f))
+    for chunk in range(n_f):
+        arrive_stream(1, chunk)
+        if chunk:
+            relayed_stream(1, chunk - 1)
     relayed_stream(1, n_f - 1)
     rescale(1)
-    for chunk in range(n_a):
+    for chunk in everything:
         gate_rows(chunk, 0, split)
         convolve(1, 1, chunk, HALO, spans[1][1][1])
         receive_halo(1, chunk)
@@ -723,18 +737,12 @@
             send_stats(1, 1)
         send_centred(1, 1, 5, chunk)
     out_copy(1).wait()
-    mix_own(1, 0)
-    mix_sibling(1, 0, 4)
-    arrived_activated(1, 0, 4)
-    mix_arrived(1, 0)
+    settle(1, 0)
+    drain(len(pending) - streamed)
+    branch(1, 0, 4)
     settle(1, 1)
-    own_activated(1, 1, 5)
-    mix_own(1, 1)
-    mix_relayed(1, 0, 4, [everything])
-    mix_sibling(1, 1, 5)
-    arrived_activated(1, 1, 5)
-    mix_arrived(1, 1)
-    mix_relayed(1, 1, 5, [(chunk,) for chunk in everything])
+    sent = len(pending)
+    branch(1, 1, 5, lambda: drain(len(pending) - sent))
 
     @pl.when(sp < n_sp - 1)
     def _():
@@ -742,8 +750,7 @@
             for chunk in range(n_a):
                 halo_copy(layer, chunk).wait_send()
 
-    for copy in pending:
-        copy.wait_send()
+    drain()
 
 
 def fused(mesh, stream, norm_gain, value_weight, gate_weight, conv_kernel, conv_bias,

time: 49.9 us -> 47.4 us (0.950)
  Pallas kernels: 48.9 us -> 46.4 us
    pallas_call x1, Pallas kernels: 48.9 us -> 46.4 us  [fused(): pl.pallas_call(functools.partial(kernel, n_tp, n_sp, split), out_shape=ja...]
where the time goes in v3:
time: 47.4 us; the launch traced here: 47.3 us
  Pallas kernels  46.4 us (98%)
  local copies, waits for them, and re-layouts  0.84 us (2%)
    pallas_call x1, Pallas kernels, fused(): pl.pallas_call(functools.partial(kernel, n_tp, n_sp, split), out_shape=ja...  46.4 us

profile of v3, /device:TPU:0, one launch (start us, length us, event | category | flops | bytes accessed | tf_op | source)
XLA Modules:
  0.0 47.3 jit_solution(7841145244753268517)
XLA Ops:
  0.0 46.4 %shard_map.91 = bf16[320,1024]{1,0:T(8,128)(2,1)S(1)} custom-call(bf16[320,4096]{1,0:T(8,128)(2,1)} %bitcast.4, f32[2,4096]{1,0:T(2,128)} %gain_hbm.1, f32[31,2,512]{2,1,0:T(2,128)} %bitcast.5, f32[2,512]{1,0:T(2,128)} %bias_hbm.1, f32[2,512]{1,0:T(2,128)} %chan_gain_hbm.1, f32[2,512]{1,0:T(2,128)} %chan_bias_hbm.1, bf16[2,512,4096]{2,1,0:T(8,128)(2,1)} %wv_ref.1, ...), custom_call_target="tpu_custom_call" | custom-call | tf_op jit(solution)/shard_map/pallas_call | solution.py:784
  46.4 0.8 %copy.11 = bf16[1024,320]{0,1:T(8,128)(2,1)} copy(bf16[1024,320]{0,1:T(8,128)(2,1)S(1)} %bitcast.3) | data formatting | bytes 1310720

commit v4 on v3

--- a/solution.py
+++ b/solution.py
@@ -130,7 +130,7 @@
     ow_ref,
     out_ref,
     gain_ref,
-    raw_taps,
+    taps,
     bias_ref,
     chan,
     wp,
@@ -139,7 +139,6 @@
     xg,
     ext,
     filt,
-    taps,
     norm_squares,
     scale,
     part,
@@ -158,17 +157,19 @@
     x_sem,
     wp_sem,
     wo_sem,
-    chan_send,
+    y_sent,
+    own_sent,
+    f_sent,
+    stat_sent,
+    square_sent,
+    chan_sent,
+    halo_sent,
     chan_recv,
-    halo_send,
     halo_recv,
-    stat_send,
     stat_recv,
-    square_send,
     square_recv,
-    y_send,
     y_recv,
-    f_send,
+    own_recv,
     f_recv,
 ):
     tokens, width = x_in.shape
@@ -194,15 +195,13 @@
 
     smalls = [
         pltpu.make_async_copy(source, target, small_sem.at[index])
-        for index, (source, target) in enumerate(
-            (
-                (gain_hbm, gain_ref),
-                (taps_hbm, raw_taps),
-                (bias_hbm, bias_ref),
-                (chan_gain_hbm, chan.at[my_y, 0]),
-                (chan_bias_hbm, chan.at[my_y, 1]),
-            )
-        )
+        for index, (source, target) in enumerate((
+            (gain_hbm, gain_ref),
+            (taps_hbm, taps),
+            (bias_hbm, bias_ref),
+            (chan_gain_hbm, chan.at[my_y, 0]),
+            (chan_bias_hbm, chan.at[my_y, 1]),
+        ))
     ]
 
     def x_copy(index):
@@ -216,7 +215,7 @@
             pltpu.make_async_copy(
                 ref.at[layer, rows, cols],
                 wp.at[layer, chunk, pl.ds(half * CHUNK, CHUNK), cols],
-                wp_sem.at[layer, chunk, index or 0],
+                wp_sem.at[layer * n_a + chunk] if index is None else x_sem.at[PIECES + index],
             )
             for half, ref in enumerate((wv_ref, wg_ref))
         ]
@@ -224,12 +223,13 @@
     def out_copy(layer):
         return pltpu.make_async_copy(ow_ref.at[layer], wo.at[layer], wo_sem.at[layer])
 
-    for copy in smalls:
-        copy.start()
+    smalls[0].start()
     for index in range(PIECES):
         x_copy(index).start()
         for copy in proj_copies(0, 0, index):
             copy.start()
+    for copy in smalls[1:]:
+        copy.start()
 
     barrier = pltpu.get_barrier_semaphore()
     for step in range(1, n_tp):
@@ -247,8 +247,6 @@
 
     part[...] = jnp.zeros(part.shape, jnp.float32)
     columns[...] = jnp.zeros(columns.shape, jnp.float32)
-
-    pending = []
 
     def remote(source, target, send, recv, device):
         return pltpu.make_async_remote_copy(
@@ -262,11 +260,9 @@
 
     def launch(copy):
         copy.start()
-        pending.append(copy)
-
-    def drain(keep=0):
-        while len(pending) > keep:
-            pending.pop(0).wait_send()
+
+    def wait_bytes(ref, semaphore):
+        pltpu.make_async_copy(ref, ref, semaphore).wait()
 
     def rows_of(span):
         return pl.ds(span[0], span[1] - span[0])
@@ -276,22 +272,28 @@
 
     def y_origin(step):
         return lax.rem(my_y + n_y - step, n_y)
+
+    def slot(phase, chunk):
+        return phase * n_a + max(0, min(phase, 4) - 2) * (n_f - n_a) + chunk
 
     def y_copy(phase, ref, step, chunk):
         target = y_peer(step) * CORES + core
         return remote(
-            ref, ref, y_send.at[phase, step, chunk], y_recv.at[phase, step, chunk], target
+            ref, ref, y_sent.at[phase, step - 1], y_recv.at[slot(phase, chunk), step - 1], target
         )
 
     def f_copy(phase, buf, step, chunk, owner, span):
         ref = buf.at[owner, chunk, rows_of(span)]
+        if step == 0:
+            return remote(ref, ref, own_sent.at[phase], own_recv.at[phase], sibling)
+        index = slot(phase, chunk)
         return remote(
-            ref, ref, f_send.at[phase, step, chunk], f_recv.at[phase, step, chunk], sibling
+            ref, ref, f_sent.at[phase, step - 1], f_recv.at[index, step - 1], sibling
         )
 
     def chan_copy(step, slot):
         target = y_peer(step) * CORES + core
-        return remote(chan.at[slot], chan.at[slot], chan_send.at[step], chan_recv.at[step], target)
+        return remote(chan.at[slot], chan.at[slot], chan_sent.at[step - 1], chan_recv.at[step - 1], target)
 
     def prepare(index):
         gains = gain_ref[0:1, index * piece : (index + 1) * piece]
@@ -335,7 +337,7 @@
         return pltpu.make_async_remote_copy(
             src_ref=halo_out.at[layer, chunk],
             dst_ref=halo_in.at[layer, chunk],
-            send_sem=halo_send.at[layer, chunk],
+            send_sem=halo_sent.at[layer],
             recv_sem=halo_recv.at[layer, chunk],
             device_id={"sp": lax.rem(sp + 1, n_sp)},
             device_id_type=MESH,
@@ -381,7 +383,7 @@
                 for residue in range(SUBLANES):
                     begin = first_row + HALO - K + 1 + residue
                     held_taps = range(residue, K, SUBLANES)
-                    weights = [taps[layer, tap : tap + 1, here] for tap in held_taps]
+                    weights = [taps[tap, layer : layer + 1, here] for tap in held_taps]
                     for index in range(tiles + len(weights) - 1):
                         at = begin + index * SUBLANES
                         window = ext[lane, at : at + SUBLANES, :]
@@ -425,7 +427,7 @@
     def stat_copy(layer, half, step, owner, target):
         ref = stat.at[layer, half, owner]
         index = layer * 2 + half
-        return remote(ref, ref, stat_send.at[index, step], stat_recv.at[index, step], target)
+        return remote(ref, ref, stat_sent.at[index], stat_recv.at[index], target)
 
     def send_stats(layer, half):
         stat[layer, half, me] = jnp.transpose(columns[half])[:SUBLANES]
@@ -437,9 +439,7 @@
         return jnp.transpose(jnp.concatenate((rows, fill), axis=0))
 
     def settle(layer, half):
-        for step in range(1, n_tp):
-            origin = lax.rem(me + n_tp - step, n_tp)
-            stat_copy(layer, half, step, origin, origin).wait_recv()
+        wait_bytes(stat.at[layer, half, pl.ds(0, n_tp - 1)], stat_recv.at[layer * 2 + half])
         totals = jnp.sum(stat[layer, half], axis=0)
         mean_row = jnp.sum(totals[:n_a], axis=0, keepdims=True) * CHUNK / total_chans
         square_row = jnp.sum(totals[n_a : 2 * n_a], axis=0, keepdims=True) / total_chans
@@ -484,7 +484,11 @@
             activate(layer, half, step, chunk)
             launch(f_copy(phase, ag.at[layer], step, chunk, owner, spans[layer][half]))
 
-    def from_sibling(layer, half, phase, chunk, step=0):
+    def from_next_door(layer, half, phase):
+        rows = rows_of(spans[layer][half])
+        wait_bytes(ag.at[layer, sibling, :, rows], own_recv.at[phase])
+
+    def from_sibling(layer, half, phase, chunk, step):
         owner = y_origin(step) * CORES + 1 - core
         f_copy(phase, ag.at[layer], step, chunk, owner, spans[layer][half]).wait_recv()
 
@@ -521,16 +525,15 @@
     def relayed(chunks):
         return [(y_origin(step) * CORES + 1 - core, chunk) for step in others for chunk in chunks]
 
-    def branch(layer, half, phase, ahead=None):
+    def branch_start(layer, half, phase):
         own_activated(layer, half, phase)
-        mix(layer, half, own(everything), True)
         for chunk in everything[:-1]:
             arrive(layer, half, phase, chunk)
-        for chunk in everything:
-            from_sibling(layer, half, phase, chunk)
-        mix(layer, half, next_door(everything) + across(everything[:-1]))
-        if ahead is not None:
-            ahead()
+        mix(layer, half, own(everything) + across(everything[:-1]), True)
+        from_next_door(layer, half, phase)
+
+    def branch_end(layer, half, phase):
+        mix(layer, half, next_door(everything))
         arrive(layer, half, phase, n_a - 1)
         for step in others:
             for chunk in everything[:-1]:
@@ -538,32 +541,59 @@
         mix(layer, half, across(everything[-1:]) + relayed(everything[:-1]))
         for step in others:
             from_sibling(layer, half, phase, n_a - 1, step)
-        mix(layer, half, relayed(everything[-1:]), False, layer == LAYERS - 1)
+
+    def sent_branch(layer, half, phase):
+        rows = rows_of(spans[layer][half])
+        wait_bytes(ag.at[layer, me, :, rows], own_sent.at[phase])
+        wait_bytes(stat.at[layer, half, pl.ds(0, n_tp - 1)], stat_sent.at[layer * 2 + half])
+        for step in others:
+            owner = y_origin(step) * CORES + core
+            wait_bytes(cf.at[layer, my_y, :, rows], y_sent.at[phase, step - 1])
+            wait_bytes(ag.at[layer, owner, :, rows], f_sent.at[phase, step - 1])
+
+    def sent_stream(half):
+        rows = rows_of(spans[0][half])
+        wait_bytes(sg.at[me, :, rows], own_sent.at[2 + half])
+        wait_bytes(square.at[half, pl.ds(0, n_tp - 1)], square_sent.at[half])
+        for step in others:
+            owner = y_origin(step) * CORES + core
+            wait_bytes(sg.at[me, :, rows], y_sent.at[2 + half, step - 1])
+            wait_bytes(sg.at[owner, :, rows], f_sent.at[2 + half, step - 1])
 
     def square_copy(half, step, owner, target):
         ref = square.at[half, owner]
-        return remote(ref, ref, square_send.at[half, step], square_recv.at[half, step], target)
+        return remote(ref, ref, square_sent.at[half], square_recv.at[half], target)
 
     def send_stream(half):
         span = spans[0][half]
         rows = slice(*span)
         squares = jnp.zeros((span[1] - span[0], LANES), jnp.float32)
-        for chunk in range(n_f):
-            first = pl.multiple_of(me * feats + chunk * CHUNK, LANES)
-            gains = gain_ref[1:2, pl.ds(first, CHUNK)]
-            for lane in range(groups):
-                cols = slice(lane * LANES, (lane + 1) * LANES)
-                here = slice(chunk * CHUNK + lane * LANES, chunk * CHUNK + (lane + 1) * LANES)
-                rounded = acco[rows, here].astype(jnp.bfloat16).astype(jnp.float32)
-                sg[me, chunk, rows, cols] = (rounded * gains[:, cols]).astype(jnp.bfloat16)
-                res[rows, here] = rounded
-                squares = squares + rounded * rounded
-            if chunk == n_f - 1:
-                send_squares(half, squares)
-            ref = sg.at[me, chunk, rows_of(span)]
-            for step in range(1, n_y):
-                launch(y_copy(2 + half, ref, step, chunk))
-            launch(f_copy(2 + half, sg, 0, chunk, me, span))
+        for lead in ((0, 1), (1, n_f)):
+            block = slice(lead[0] * CHUNK, lead[1] * CHUNK)
+            total = acco[rows, block]
+            for owner, last in relayed(everything[-1:]):
+                start = pl.multiple_of(owner * chans + last * CHUNK, LANES)
+                total = total + dot_nt(
+                    ag[0, owner, last, rows, :], wo[0, block, pl.ds(start, CHUNK)]
+                )
+            rounded = total.astype(jnp.bfloat16).astype(jnp.float32)
+            res[rows, block] = rounded
+            for chunk in range(*lead):
+                first = pl.multiple_of(me * feats + chunk * CHUNK, LANES)
+                at = (chunk - lead[0]) * CHUNK
+                values = rounded[:, at : at + CHUNK]
+                sg[me, chunk, rows, :] = (values * gain_ref[1:2, pl.ds(first, CHUNK)]).astype(
+                    jnp.bfloat16
+                )
+                for lane in range(groups):
+                    part = values[:, lane * LANES : (lane + 1) * LANES]
+                    squares = squares + part * part
+                if chunk == n_f - 1:
+                    send_squares(half, squares)
+                ref = sg.at[me, chunk, rows_of(span)]
+                for step in others:
+                    launch(y_copy(2 + half, ref, step, chunk))
+                launch(f_copy(2 + half, sg, 0, chunk, me, span))
 
     def send_squares(half, squares):
         span = spans[0][half]
@@ -577,9 +607,7 @@
             launch(square_copy(half, step, me, lax.rem(me + step, n_tp)))
 
     def rescale(half):
-        for step in range(1, n_tp):
-            origin = lax.rem(me + n_tp - step, n_tp)
-            square_copy(half, step, origin, origin).wait_recv()
+        wait_bytes(square.at[half, pl.ds(0, n_tp - 1)], square_recv.at[half])
         totals = jnp.sum(square[half], axis=0)[0:1] / width
         start, stop = spans[0][half]
         spread = jnp.transpose(
@@ -587,9 +615,9 @@
         )
         scale[start:stop, :] = spread[: stop - start]
 
-    def project(half, owner, chunks, first):
+    def project(half, owner, chunks, first, blocks=None):
         rows = slice(*spans[0][half])
-        for block in range(n_a):
+        for block in range(n_a) if blocks is None else blocks:
             total = None if first else accp[rows, held(block)]
             for chunk in chunks:
                 start = pl.multiple_of(owner * feats + chunk * CHUNK, LANES)
@@ -603,8 +631,7 @@
         project(half, me, range(n_f), True)
 
     def sibling_stream(half):
-        for chunk in range(n_f):
-            f_copy(2 + half, sg, 0, chunk, sibling, spans[0][half]).wait_recv()
+        wait_bytes(sg.at[sibling, :, rows_of(spans[0][half])], own_recv.at[2 + half])
         project(half, sibling, range(n_f), False)
 
     def arrive_stream(half, chunk):
@@ -616,16 +643,14 @@
             launch(f_copy(2 + half, sg, step, chunk, owner, spans[0][half]))
             project(half, owner, (chunk,), False)
 
-    def relayed_stream(half, chunk):
-        for step in range(1, n_y):
+    def relayed_stream(half, chunk, blocks=None):
+        for step in others:
             owner = y_origin(step) * CORES + 1 - core
-            f_copy(2 + half, sg, step, chunk, owner, spans[0][half]).wait_recv()
-            project(half, owner, (chunk,), False)
-
-    for copy in smalls:
-        copy.wait()
-    for layer in range(LAYERS):
-        taps[layer] = raw_taps[:, layer, :]
+            if blocks is None or blocks[0] == 0:
+                f_copy(2 + half, sg, step, chunk, owner, spans[0][half]).wait_recv()
+            project(half, owner, (chunk,), False, blocks)
+
+    smalls[0].wait()
     x_copy(0).wait()
     prepare(0)
     for index in range(PIECES):
@@ -651,6 +676,8 @@
         scaling = lax.rsqrt(jnp.sum(norm_squares[rows, :], axis=1, keepdims=True) / width + epsilon)
         scale[rows, :] = jnp.broadcast_to(0.5 * scaling, (ROWS, LANES))
 
+    for copy in smalls[1:]:
+        copy.wait()
     pl.semaphore_wait(
         barrier,
         n_tp - 1 + jnp.where(sp > 0, 1, 0) + jnp.where(sp < n_sp - 1, 1, 0),
@@ -688,11 +715,12 @@
         chan_copy(step, y_origin(step)).wait_recv()
     out_copy(0).wait()
     settle(0, 0)
-    branch(0, 0, 0)
+    branch_start(0, 0, 0)
+    branch_end(0, 0, 0)
     send_stream(0)
     settle(0, 1)
-    branch(0, 1, 1)
-    settled = len(pending)
+    branch_start(0, 1, 1)
+    branch_end(0, 1, 1)
     send_stream(1)
     part[...] = jnp.zeros(part.shape, jnp.float32)
     for chunk in everything:
@@ -706,28 +734,29 @@
         if chunk == 2:
             sibling_stream(1)
         if chunk == n_f - 1:
-            drain(len(pending) - settled)
+            sent_branch(0, 0, 0)
+            sent_branch(0, 1, 1)
+            rescale(0)
         arrive_stream(0, chunk)
         if chunk:
             relayed_stream(0, chunk - 1)
-    relayed_stream(0, n_f - 1)
-    rescale(0)
     for chunk in everything:
+        relayed_stream(0, n_f - 1, (chunk,))
         send_halo(1, chunk)
         gate_rows(chunk, split, tokens - HALO)
         convolve(1, 0, chunk, *spans[1][0])
         centre(1, 0, chunk)
-    streamed = len(pending)
     send_stats(1, 0)
     for chunk in everything:
         send_centred(1, 0, 4, chunk)
     for chunk in range(n_f):
+        if chunk == n_f - 1:
+            rescale(1)
         arrive_stream(1, chunk)
         if chunk:
             relayed_stream(1, chunk - 1)
-    relayed_stream(1, n_f - 1)
-    rescale(1)
     for chunk in everything:
+        relayed_stream(1, n_f - 1, (chunk,))
         gate_rows(chunk, 0, split)
         convolve(1, 1, chunk, HALO, spans[1][1][1])
         receive_halo(1, chunk)
@@ -738,19 +767,31 @@
         send_centred(1, 1, 5, chunk)
     out_copy(1).wait()
     settle(1, 0)
-    drain(len(pending) - streamed)
-    branch(1, 0, 4)
+    own_activated(1, 0, 4)
+    for chunk in everything:
+        arrive(1, 0, 4, chunk)
+    mix(1, 0, own(everything) + across(everything), True)
+    from_next_door(1, 0, 4)
+    for chunk in everything:
+        for step in others:
+            from_sibling(1, 0, 4, chunk, step)
+    mix(1, 0, next_door(everything) + relayed(everything), False, True)
+    sent_stream(0)
+    sent_stream(1)
     settle(1, 1)
-    sent = len(pending)
-    branch(1, 1, 5, lambda: drain(len(pending) - sent))
+    branch_start(1, 1, 5)
+    sent_branch(1, 0, 4)
+    branch_end(1, 1, 5)
+    mix(1, 1, relayed(everything[-1:]), False, True)
 
     @pl.when(sp < n_sp - 1)
     def _():
         for layer in range(LAYERS):
-            for chunk in range(n_a):
-                halo_copy(layer, chunk).wait_send()
-
-    drain()
+            wait_bytes(halo_out.at[layer], halo_sent.at[layer])
+
+    sent_branch(1, 1, 5)
+    for step in others:
+        wait_bytes(chan.at[my_y], chan_sent.at[step - 1])
 
 
 def fused(mesh, stream, norm_gain, value_weight, gate_weight, conv_kernel, conv_bias,
@@ -778,7 +819,6 @@
         return local(stream, norm_gain, value_weight, gate_weight, conv_kernel, conv_bias,
                      channel_gain, channel_bias, out_weight)
     padded = -(-(tokens - split) // LANES) * LANES
-    most = max(n_a, n_f)
     f32, bf16 = jnp.float32, jnp.bfloat16
     dma = pltpu.SemaphoreType.DMA
     out = pl.pallas_call(
@@ -797,7 +837,6 @@
             pltpu.VMEM((tokens, width), bf16),
             pltpu.VMEM((chans // LANES, HALO + tokens, LANES), f32),
             pltpu.VMEM((tokens, chans), f32),
-            pltpu.VMEM((LAYERS, K, chans), f32),
             pltpu.VMEM((tokens, LANES), f32),
             pltpu.VMEM((tokens, LANES), f32),
             pltpu.VMEM((2, n_a, 2, padded, LANES), f32),
@@ -813,21 +852,23 @@
             pltpu.VMEM((tokens, feats), f32),
             pltpu.VMEM((tokens, feats), f32),
             dma((5,)),
-            dma((PIECES,)),
-            dma((LAYERS, n_a, PIECES)),
+            dma((2 * PIECES,)),
+            dma((LAYERS * n_a,)),
             dma((LAYERS,)),
-            dma((n_y,)),
-            dma((n_y,)),
+            dma((6, n_y - 1)),
+            dma((6,)),
+            dma((6, n_y - 1)),
+            dma((LAYERS * 2,)),
+            dma((2,)),
+            dma((n_y - 1,)),
+            dma((LAYERS,)),
+            dma((n_y - 1,)),
             dma((LAYERS, n_a)),
-            dma((LAYERS, n_a)),
-            dma((LAYERS * 2, n_tp)),
-            dma((LAYERS * 2, n_tp)),
-            dma((2, n_tp)),
-            dma((2, n_tp)),
-            dma((6, n_y, most)),
-            dma((6, n_y, most)),
-            dma((6, n_y, most)),
-            dma((6, n_y, most)),
+            dma((LAYERS * 2,)),
+            dma((2,)),
+            dma((4 * n_a + 2 * n_f, n_y - 1)),
+            dma((6,)),
+            dma((4 * n_a + 2 * n_f, n_y - 1)),
         ],
         compiler_params=pltpu.CompilerParams(
             collective_id=0, has_side_effects=True, vmem_limit_bytes=50 * 1024 * 1024

time: 47.4 us -> 44.8 us (0.945)
  Pallas kernels: 46.4 us -> 43.9 us
    pallas_call x1, Pallas kernels: 46.4 us -> 43.9 us  [fused(): pl.pallas_call(functools.partial(kernel, n_tp, n_sp, split), out_shape=ja...]
where the time goes in v4:
time: 44.8 us; the launch traced here: 44.7 us
  Pallas kernels  43.9 us (98%)
  local copies, waits for them, and re-layouts  0.84 us (2%)
    pallas_call x1, Pallas kernels, fused(): pl.pallas_call(functools.partial(kernel, n_tp, n_sp, split), out_shape=ja...  43.9 us

profile of v4, /device:TPU:0, one launch (start us, length us, event | category | flops | bytes accessed | tf_op | source)
XLA Modules:
  0.0 44.7 jit_solution(4726484703138995557)
XLA Ops:
  0.0 43.9 %shard_map.91 = bf16[320,1024]{1,0:T(8,128)(2,1)S(1)} custom-call(bf16[320,4096]{1,0:T(8,128)(2,1)} %bitcast.4, f32[2,4096]{1,0:T(2,128)} %gain_hbm.1, f32[31,2,512]{2,1,0:T(2,128)} %bitcast.5, f32[2,512]{1,0:T(2,128)} %bias_hbm.1, f32[2,512]{1,0:T(2,128)} %chan_gain_hbm.1, f32[2,512]{1,0:T(2,128)} %chan_bias_hbm.1, bf16[2,512,4096]{2,1,0:T(8,128)(2,1)} %wv_ref.1, ...), custom_call_target="tpu_custom_call" | custom-call | tf_op jit(solution)/shard_map/pallas_call | solution.py:824
  43.9 0.8 %copy.11 = bf16[1024,320]{0,1:T(8,128)(2,1)} copy(bf16[1024,320]{0,1:T(8,128)(2,1)S(1)} %bitcast.3) | data formatting | bytes 1310720

commit v5 on v4

--- a/solution.py
+++ b/solution.py
@@ -157,9 +157,7 @@
     x_sem,
     wp_sem,
     wo_sem,
-    y_sent,
-    own_sent,
-    f_sent,
+    sent,
     stat_sent,
     square_sent,
     chan_sent,
@@ -179,6 +177,7 @@
     n_y = n_tp // CORES
     piece = width // PIECES
     padded = stat.shape[-1]
+    stat_rows = stat.shape[-2]
     n_a, n_f = chans // CHUNK, feats // CHUNK
     groups = CHUNK // LANES
     spans = (
@@ -267,6 +266,15 @@
     def rows_of(span):
         return pl.ds(span[0], span[1] - span[0])
 
+    def columns_of(span):
+        return pl.ds(0, -(-(span[1] - span[0]) // LANES) * LANES)
+
+    def stats_of(layer, half):
+        return stat.at[layer, half, pl.ds(0, n_tp - 1), :, columns_of(spans[layer][half])]
+
+    def squares_of(half):
+        return square.at[half, pl.ds(0, n_tp - 1), :, columns_of(spans[0][half])]
+
     def y_peer(step):
         return lax.rem(my_y + step, n_y)
 
@@ -279,16 +287,16 @@
     def y_copy(phase, ref, step, chunk):
         target = y_peer(step) * CORES + core
         return remote(
-            ref, ref, y_sent.at[phase, step - 1], y_recv.at[slot(phase, chunk), step - 1], target
+            ref, ref, sent.at[phase], y_recv.at[slot(phase, chunk), step - 1], target
         )
 
     def f_copy(phase, buf, step, chunk, owner, span):
         ref = buf.at[owner, chunk, rows_of(span)]
         if step == 0:
-            return remote(ref, ref, own_sent.at[phase], own_recv.at[phase], sibling)
+            return remote(ref, ref, sent.at[phase], own_recv.at[phase], sibling)
         index = slot(phase, chunk)
         return remote(
-            ref, ref, f_sent.at[phase, step - 1], f_recv.at[index, step - 1], sibling
+            ref, ref, sent.at[phase], f_recv.at[index, step - 1], sibling
         )
 
     def chan_copy(step, slot):
@@ -425,12 +433,12 @@
             launch(y_copy(phase, ref, step, chunk))
 
     def stat_copy(layer, half, step, owner, target):
-        ref = stat.at[layer, half, owner]
+        ref = stat.at[layer, half, owner, :, columns_of(spans[layer][half])]
         index = layer * 2 + half
         return remote(ref, ref, stat_sent.at[index], stat_recv.at[index], target)
 
     def send_stats(layer, half):
-        stat[layer, half, me] = jnp.transpose(columns[half])[:SUBLANES]
+        stat[layer, half, me] = jnp.transpose(columns[half])[:stat_rows]
         for step in range(1, n_tp):
             launch(stat_copy(layer, half, step, me, lax.rem(me + step, n_tp)))
 
@@ -439,7 +447,7 @@
         return jnp.transpose(jnp.concatenate((rows, fill), axis=0))
 
     def settle(layer, half):
-        wait_bytes(stat.at[layer, half, pl.ds(0, n_tp - 1)], stat_recv.at[layer * 2 + half])
+        wait_bytes(stats_of(layer, half), stat_recv.at[layer * 2 + half])
         totals = jnp.sum(stat[layer, half], axis=0)
         mean_row = jnp.sum(totals[:n_a], axis=0, keepdims=True) * CHUNK / total_chans
         square_row = jnp.sum(totals[n_a : 2 * n_a], axis=0, keepdims=True) / total_chans
@@ -530,38 +538,35 @@
         for chunk in everything[:-1]:
             arrive(layer, half, phase, chunk)
         mix(layer, half, own(everything) + across(everything[:-1]), True)
-        from_next_door(layer, half, phase)
-
-    def branch_end(layer, half, phase):
-        mix(layer, half, next_door(everything))
+
+    def branch_end(layer, half, phase, early=False):
+        parts = next_door(everything)
+        if not early:
+            from_next_door(layer, half, phase)
+            mix(layer, half, parts)
+            parts = []
         arrive(layer, half, phase, n_a - 1)
+        if early:
+            from_next_door(layer, half, phase)
         for step in others:
             for chunk in everything[:-1]:
                 from_sibling(layer, half, phase, chunk, step)
-        mix(layer, half, across(everything[-1:]) + relayed(everything[:-1]))
+        mix(layer, half, parts + across(everything[-1:]) + relayed(everything[:-1]))
         for step in others:
             from_sibling(layer, half, phase, n_a - 1, step)
 
     def sent_branch(layer, half, phase):
         rows = rows_of(spans[layer][half])
-        wait_bytes(ag.at[layer, me, :, rows], own_sent.at[phase])
-        wait_bytes(stat.at[layer, half, pl.ds(0, n_tp - 1)], stat_sent.at[layer * 2 + half])
-        for step in others:
-            owner = y_origin(step) * CORES + core
-            wait_bytes(cf.at[layer, my_y, :, rows], y_sent.at[phase, step - 1])
-            wait_bytes(ag.at[layer, owner, :, rows], f_sent.at[phase, step - 1])
+        wait_bytes(ag.at[layer, pl.ds(0, 2 * n_y - 1), :, rows], sent.at[phase])
+        wait_bytes(stats_of(layer, half), stat_sent.at[layer * 2 + half])
 
     def sent_stream(half):
         rows = rows_of(spans[0][half])
-        wait_bytes(sg.at[me, :, rows], own_sent.at[2 + half])
-        wait_bytes(square.at[half, pl.ds(0, n_tp - 1)], square_sent.at[half])
-        for step in others:
-            owner = y_origin(step) * CORES + core
-            wait_bytes(sg.at[me, :, rows], y_sent.at[2 + half, step - 1])
-            wait_bytes(sg.at[owner, :, rows], f_sent.at[2 + half, step - 1])
+        wait_bytes(sg.at[pl.ds(0, 2 * n_y - 1), :, rows], sent.at[2 + half])
+        wait_bytes(squares_of(half), square_sent.at[half])
 
     def square_copy(half, step, owner, target):
-        ref = square.at[half, owner]
+        ref = square.at[half, owner, :, columns_of(spans[0][half])]
         return remote(ref, ref, square_sent.at[half], square_recv.at[half], target)
 
     def send_stream(half):
@@ -602,13 +607,13 @@
             fill = jnp.zeros((padded - count, LANES), jnp.float32)
             squares = jnp.concatenate((squares, fill), axis=0)
         row = jnp.sum(jnp.transpose(squares), axis=0, keepdims=True)
-        square[half, me] = jnp.broadcast_to(row, (SUBLANES, padded))
+        square[half, me] = row
         for step in range(1, n_tp):
             launch(square_copy(half, step, me, lax.rem(me + step, n_tp)))
 
     def rescale(half):
-        wait_bytes(square.at[half, pl.ds(0, n_tp - 1)], square_recv.at[half])
-        totals = jnp.sum(square[half], axis=0)[0:1] / width
+        wait_bytes(squares_of(half), square_recv.at[half])
+        totals = jnp.sum(square[half], axis=0) / width
         start, stop = spans[0][half]
         spread = jnp.transpose(
             jnp.broadcast_to(0.5 * lax.rsqrt(totals + epsilon), (LANES, padded))
@@ -663,6 +668,7 @@
             for chunk in range(1, n_a):
                 for copy in proj_copies(0, chunk):
                     copy.start()
+            out_copy(0).start()
         product = dot_nt(xg[:, cols], wp[0, 0, :, cols])
         if index < PIECES - 1:
             prepare(index + 1)
@@ -698,7 +704,6 @@
         if chunk == 0:
             for step in others:
                 launch(chan_copy(step, my_y))
-    out_copy(0).start()
     for chunk in everything:
         convolve(0, 1, chunk, ROWS, spans[0][1][1])
         receive_halo(0, chunk)
@@ -781,7 +786,7 @@
     settle(1, 1)
     branch_start(1, 1, 5)
     sent_branch(1, 0, 4)
-    branch_end(1, 1, 5)
+    branch_end(1, 1, 5, True)
     mix(1, 1, relayed(everything[-1:]), False, True)
 
     @pl.when(sp < n_sp - 1)
@@ -843,8 +848,8 @@
             pltpu.VMEM((2, padded, LANES), f32),
             pltpu.VMEM((LAYERS, n_a, HALO, CHUNK), bf16),
             pltpu.VMEM((LAYERS, n_a, HALO, CHUNK), bf16),
-            pltpu.VMEM((LAYERS, 2, n_tp, SUBLANES, padded), f32),
-            pltpu.VMEM((2, n_tp, SUBLANES, padded), f32),
+            pltpu.VMEM((LAYERS, 2, n_tp, 4 if 2 * n_a <= 4 else SUBLANES, padded), f32),
+            pltpu.VMEM((2, n_tp, 1, padded), f32),
             pltpu.VMEM((LAYERS, n_y, n_a, tokens, CHUNK), bf16),
             pltpu.VMEM((LAYERS, n_tp, n_a, tokens, CHUNK), bf16),
             pltpu.VMEM((n_tp, n_f, tokens, CHUNK), bf16),
@@ -855,9 +860,7 @@
             dma((2 * PIECES,)),
             dma((LAYERS * n_a,)),
             dma((LAYERS,)),
-            dma((6, n_y - 1)),
             dma((6,)),
-            dma((6, n_y - 1)),
             dma((LAYERS * 2,)),
             dma((2,)),
             dma((n_y - 1,)),

time: 44.8 us -> 43.6 us (0.973)
  Pallas kernels: 43.9 us -> 42.6 us
    pallas_call x1, Pallas kernels: 43.9 us -> 42.6 us  [fused(): pl.pallas_call(functools.partial(kernel, n_tp, n_sp, split), out_shape=ja...]
where the time goes in v5:
time: 43.6 us; the launch traced here: 43.5 us
  Pallas kernels  42.6 us (98%)
  local copies, waits for them, and re-layouts  0.84 us (2%)
    pallas_call x1, Pallas kernels, fused(): pl.pallas_call(functools.partial(kernel, n_tp, n_sp, split), out_shape=ja...  42.6 us

profile of v5, /device:TPU:0, one launch (start us, length us, event | category | flops | bytes accessed | tf_op | source)
XLA Modules:
  0.0 43.5 jit_solution(224383276145936514)
XLA Ops:
  0.0 42.6 %shard_map.91 = bf16[320,1024]{1,0:T(8,128)(2,1)S(1)} custom-call(bf16[320,4096]{1,0:T(8,128)(2,1)} %bitcast.4, f32[2,4096]{1,0:T(2,128)} %gain_hbm.1, f32[31,2,512]{2,1,0:T(2,128)} %bitcast.5, f32[2,512]{1,0:T(2,128)} %bias_hbm.1, f32[2,512]{1,0:T(2,128)} %chan_gain_hbm.1, f32[2,512]{1,0:T(2,128)} %chan_bias_hbm.1, bf16[2,512,4096]{2,1,0:T(8,128)(2,1)} %wv_ref.1, ...), custom_call_target="tpu_custom_call" | custom-call | tf_op jit(solution)/shard_map/pallas_call | solution.py:829
  42.6 0.8 %copy.11 = bf16[1024,320]{0,1:T(8,128)(2,1)} copy(bf16[1024,320]{0,1:T(8,128)(2,1)S(1)} %bitcast.3) | data formatting | bytes 1310720

commit v6 on v5

--- a/solution.py
+++ b/solution.py
@@ -337,9 +337,8 @@
         return pieces
 
     def gate_rows(chunk, start, stop):
-        @pl.loop(0, (stop - start) // HALO)
-        def _(block):
-            gate(chunk, pl.multiple_of(start + block * HALO, HALO), HALO)
+        for first_row in range(start, stop, HALO):
+            gate(chunk, first_row, HALO)
 
     def halo_copy(layer, chunk):
         return pltpu.make_async_remote_copy(

time: 43.6 us -> 43.4 us (level)
  no operation moved by 1% of the time
where the time goes in v6:
time: 43.4 us; the launch traced here: 43.3 us
  Pallas kernels  42.4 us (98%)
  local copies, waits for them, and re-layouts  0.84 us (2%)
    pallas_call x1, Pallas kernels, fused(): pl.pallas_call(functools.partial(kernel, n_tp, n_sp, split), out_shape=ja...  42.4 us

profile of v6, /device:TPU:0, one launch (start us, length us, event | category | flops | bytes accessed | tf_op | source)
XLA Modules:
  0.0 43.3 jit_solution(15542067240392459566)
XLA Ops:
  0.0 42.4 %shard_map.91 = bf16[320,1024]{1,0:T(8,128)(2,1)S(1)} custom-call(bf16[320,4096]{1,0:T(8,128)(2,1)} %bitcast.4, f32[2,4096]{1,0:T(2,128)} %gain_hbm.1, f32[31,2,512]{2,1,0:T(2,128)} %bitcast.5, f32[2,512]{1,0:T(2,128)} %bias_hbm.1, f32[2,512]{1,0:T(2,128)} %chan_gain_hbm.1, f32[2,512]{1,0:T(2,128)} %chan_bias_hbm.1, bf16[2,512,4096]{2,1,0:T(8,128)(2,1)} %wv_ref.1, ...), custom_call_target="tpu_custom_call" | custom-call | tf_op jit(solution)/shard_map/pallas_call | solution.py:828
  42.5 0.8 %copy.11 = bf16[1024,320]{0,1:T(8,128)(2,1)} copy(bf16[1024,320]{0,1:T(8,128)(2,1)S(1)} %bitcast.3) | data formatting | bytes 1310720
